TPU v7x, 32 devices: a whole 2x2x4 slice. The times are simulated.
32 devices in a mesh: kv: 8 (over z, x), tp: 4 (over y, core).
Axes of the slice: x: 2, y: 2, z: 4, core: 2. Of those that a mesh axis runs over, the one named last changes fastest.
Arguments:
- tokens: bfloat16 [384, 2048], P(None, 'kv'), may hold values from -40 to 40
- norm_gain: float32 [2048], P('kv'), may hold values from 0.1 to 1.9
- w_query: bfloat16 [2048, 1024], P('kv', 'tp'), may hold values from -0.088388348 to 0.088388348
- w_key: bfloat16 [2048, 1024], P('kv', 'tp'), may hold values from -0.125 to 0.125
- w_value: bfloat16 [2048, 1024], P('kv', 'tp'), may hold values from -0.125 to 0.125
- w_gate: bfloat16 [2048, 16], replicated, may hold values from -0.125 to 0.125
- gate_bias: float32 [16], replicated, may hold values from -1 to 3
- w_out: bfloat16 [1024, 2048], P('tp', 'kv'), may hold values from -0.1875 to 0.1875
- keys_cache: bfloat16 [24, 4096, 1024], P(None, 'kv', 'tp'), may hold values from -512 to 512
- values_cache: bfloat16 [24, 4096, 1024], P(None, 'kv', 'tp'), may hold values from -6 to 6
- cum_gates: float32 [24, 16, 4096], P(None, 'tp', 'kv'), may hold values from -4496 to 0, as said below
- prior_len: int32 [24], replicated, may hold values from 2048 to 4074, as said below
- accepted: int32 [24], replicated, may hold values from 0 to 6
- parents: int32 [24, 16], replicated, may hold values from -1 to 14, as said below
Outputs:
- mixed_rows: bfloat16 [384, 2048], P('tp', 'kv')
- keys_out: bfloat16 [24, 4096, 1024], P(None, 'kv', 'tp')
- values_out: bfloat16 [24, 4096, 1024], P(None, 'kv', 'tp')
Inputs may be any that keep to these rules, and one draw needn't show every extreme that they name: parents[b, 0] = -1 and 0 <= parents[b, j] < j for later j. prior_len is at least half of 4096, and prior_len + accepted + 16 <= 4096. `cum_gates`: non-increasing along positions.
All inputs are finite; a program needn't handle non-finite values.
Results may differ from a plain program's by a relative error of at most 0.04.
Values may be sent and summed in bfloat16 or wider, within the bound.
A program may use at most 64 MiB of HBM per device.

v0:
```python
import functools

import jax
import jax.numpy as jnp
from jax import lax
from jax.experimental import pallas as pl
from jax.experimental.pallas import tpu as pltpu
from jax.sharding import PartitionSpec as P

HEAD = 64
PROPS = 16
LANES = 128
SQUARE_LANE = 96
masked_score = -1e30
norm_eps = 1e-06
MESH = pl.DeviceIdType.MESH
HIGHEST = lax.Precision.HIGHEST
f32, bf16, i32 = jnp.float32, jnp.bfloat16, jnp.int32


def iota(shape, axis):
    return lax.broadcasted_iota(i32, shape, axis)


def split3(x):
    hi = x.astype(bf16).astype(f32)
    mid = (x - hi).astype(bf16).astype(f32)
    return hi, mid, x - hi - mid


def contract_last(a, b, precision=None):
    return lax.dot_general(
        a, b, (((1,), (1,)), ((), ())), preferred_element_type=f32, precision=precision
    )


def project_kernel(
    n_kv,
    heads,
    tokens_ref,
    gain_ref,
    wq_ref,
    wk_ref,
    wv_ref,
    wg_ref,
    bias_ref,
    out_ref,
    part,
    swapped,
    middle,
    arrived,
    gathered,
    mine,
    *sems,
):
    swap_sems, sum_sems, back_sems, last_sems = sems[0:2], sems[2:4], sems[4:6], sems[6:8]
    me = lax.axis_index("kv")
    tp = lax.axis_index("tp")
    chunk_rows, depth = tokens_ref.shape[1:]
    width = heads * HEAD
    barrier = pltpu.get_barrier_semaphore()
    for d in range(1, n_kv):
        pl.semaphore_signal(
            barrier, inc=1, device_id={"kv": lax.rem(me + d, n_kv)}, device_id_type=MESH
        )

    total_heads = bias_ref.shape[1]
    lane = iota((total_heads, LANES), 1)
    pick = (iota((total_heads, LANES), 0) == tp * heads + lane % 32) & (lane % 32 < heads) & (lane < 96)
    pick = jnp.where(pick, 1.0, 0.0)
    if depth % LANES == 0:
        slot = iota((LANES, total_heads), 0)
        pick_rows = iota((LANES, total_heads), 1) == tp * heads + slot % 32
        pick_rows = jnp.where(pick_rows & (slot % 32 < heads) & (slot < 96), 1.0, 0.0)
        gate_w = wg_ref[:, pl.ds(pl.multiple_of(me * depth, depth), depth)]
        gate_w = jnp.dot(pick_rows.astype(bf16), gate_w, preferred_element_type=f32).astype(bf16)
        gate_product = functools.partial(contract_last, b=gate_w)
    else:
        gate_w = wg_ref[pl.ds(pl.multiple_of(me * depth, depth), depth), :]
        gate_w = jnp.dot(gate_w, pick.astype(bf16), preferred_element_type=f32).astype(bf16)
        gate_product = functools.partial(jnp.dot, b=gate_w, preferred_element_type=f32)

    def partial_sums(floats):
        scaled = (floats * gain_ref[...]).astype(bf16)
        square = jnp.sum(floats * floats, axis=1, keepdims=True)
        gates = gate_product(scaled)
        gates = jnp.where(iota(gates.shape, 1) == SQUARE_LANE, square, gates)
        products = [
            jnp.dot(scaled, w[...], preferred_element_type=f32).astype(bf16)
            for w in (wq_ref, wk_ref, wv_ref)
        ]
        return products + [gates.astype(bf16)]

    edges = [0, width, 2 * width, 3 * width, 3 * width + LANES]
    if chunk_rows % 16 == 0:
        floats = tokens_ref[...].reshape(n_kv * chunk_rows, depth).astype(f32)
        for piece, low, high in zip(partial_sums(floats), edges[:-1], edges[1:]):
            blocks = piece.reshape(n_kv, chunk_rows, high - low)
            for c in range(n_kv):
                part[c % 2, c // 2, :, low:high] = blocks[c]
    else:

        def one(c, carry):
            for piece, low, high in zip(
                partial_sums(tokens_ref[c].astype(f32)), edges[:-1], edges[1:]
            ):
                part[lax.rem(c, 2), c // 2, :, low:high] = piece
            return carry

        lax.fori_loop(0, n_kv, one, 0)

    outer = n_kv // 2
    x, z = lax.rem(me, 2), me // 2
    partner = me + 1 - 2 * x
    pieces = [pl.ds(2 * width, width + LANES), pl.ds(0, width), pl.ds(width, width)]

    def send(source, target, sems, at, device):
        copy = pltpu.make_async_remote_copy(
            src_ref=source,
            dst_ref=target,
            send_sem=sems[0].at[at],
            recv_sem=sems[1].at[at],
            device_id={"kv": device},
            device_id_type=MESH,
        )
        copy.start()
        return copy

    pl.semaphore_wait(barrier, n_kv - 1)
    swaps = [
        send(part.at[1 - x, :, :, at], swapped.at[:, :, at], swap_sems, p, partner)
        for p, at in enumerate(pieces)
    ]
    sums = []
    for p, at in enumerate(pieces):
        swaps[p].wait_recv()
        half = part[x, :, :, at].astype(f32) + swapped[:, :, at].astype(f32)
        middle[:, :, at] = half.astype(bf16)
        row = []
        for d in range(1, outer):
            other = lax.rem(z + d, outer)
            row.append(
                send(
                    middle.at[other, :, at],
                    arrived.at[d - 1, :, at],
                    sum_sems,
                    p * (outer - 1) + d - 1,
                    other * 2 + x,
                )
            )
        sums.append(row)
    bias = jnp.dot(
        jnp.broadcast_to(bias_ref[...], (8, total_heads)),
        pick,
        preferred_element_type=f32,
        precision=HIGHEST,
    )[0:1]
    inv_rms = None
    backs = []
    for p, at in enumerate(pieces):
        total = middle[z, :, at].astype(f32)
        for d in range(1, outer):
            sums[p][d - 1].wait_recv()
            total = total + arrived[d - 1, :, at].astype(f32)
        if p == 0:
            tail = total[:, width:]
            tail_lane = iota(tail.shape, 1)
            square = jnp.sum(jnp.where(tail_lane == SQUARE_LANE, tail, 0.0), axis=1, keepdims=True)
            inv_rms = lax.rsqrt(square / (n_kv * depth) + norm_eps)
            pre = inv_rms * tail + bias
            log_gates = jnp.minimum(pre, 0.0) - jnp.log1p(jnp.exp(-jnp.abs(pre)))
            hi, mid, low = split3(log_gates)
            packed = jnp.where(tail_lane < 32, hi, jnp.where(tail_lane < 64, mid, low))
            packed = jnp.where((tail_lane % 32 < heads) & (tail_lane < 96), packed, 0.0)
            mine[:, 3 * width :] = packed.astype(bf16)
            total = total[:, :width]
        mine[:, pl.ds(at.start, width)] = (inv_rms * total).astype(bf16)
        backs.append(
            [
                send(
                    mine.at[:, at],
                    gathered.at[x, z, :, at],
                    back_sems,
                    p * (outer - 1) + d - 1,
                    lax.rem(z + d, outer) * 2 + x,
                )
                for d in range(1, outer)
            ]
        )
        gathered[x, z, :, at] = mine[:, at]
    lasts = []
    for p, at in enumerate(pieces):
        for copy in backs[p]:
            copy.wait_recv()
        lasts.append(
            send(gathered.at[x, :, :, at], gathered.at[x, :, :, at], last_sems, p, partner)
        )
    for copy in lasts:
        copy.wait_recv()
    for c in range(n_kv):
        out_ref[c] = gathered[c % 2, c // 2]
    for copy in swaps + sum(sums, []) + sum(backs, []) + lasts:
        copy.wait_send()


def attend_kernel(
    heads, prior_s, accepted_s, proj_ref, parents_ref, k_ref, v_ref, cum_ref, ko_ref, vo_ref, out_ref
):
    group = k_ref.shape[0]
    length = k_ref.shape[1]
    width = heads * HEAD
    rows = group * PROPS
    score_rows = heads * PROPS
    offset = lax.axis_index("kv") * length
    step = pl.program_id(0)

    row = iota((rows, rows), 0)
    column = iota((rows, rows), 1)
    every = parents_ref[...]
    parent = jnp.concatenate(
        [
            jnp.sum(
                jnp.where(iota(every.shape, 1) == step * group + b, every, 0).astype(f32),
                axis=1,
                keepdims=True,
            ).astype(i32)
            for b in range(group)
        ],
        axis=0,
    )
    link = (parent + (row // PROPS) * PROPS == column) & (parent >= 0)
    reached = jnp.where(link | (row == column), 1.0, 0.0)
    for squaring in range((PROPS - 1).bit_length()):
        reached = jnp.minimum(
            jnp.dot(reached.astype(bf16), reached.astype(bf16), preferred_element_type=f32), 1.0
        )
    tree_gates = jnp.dot(
        reached.astype(bf16), proj_ref[:, 3 * width :], preferred_element_type=f32
    )
    lane = iota((score_rows, LANES), 1)
    row_head = iota((score_rows, LANES), 0) // PROPS
    gate_pick = jnp.where((lane % 32 == row_head) & (lane < 96), 1.0, 0.0)
    same_head = iota((score_rows, width), 0) // PROPS == iota((score_rows, width), 1) // HEAD
    position = iota((score_rows, length), 1)
    window = 2 * PROPS
    for b in range(group):
        span = slice(b * PROPS, (b + 1) * PROPS)
        seq = step * group + b
        limit = prior_s[seq] + accepted_s[seq] - offset
        owner = jnp.where((limit >= 1) & (limit <= length), 1.0, 0.0)
        new_k = proj_ref[span, width : 2 * width]
        new_v = proj_ref[span, 2 * width : 3 * width]
        query = jnp.concatenate([proj_ref[span, :width]] * heads, axis=0).astype(f32)
        query = (jnp.where(same_head, query, 0.0) * HEAD ** (-0.5)).astype(bf16)
        cum = jnp.concatenate(
            [
                jnp.broadcast_to(cum_ref[b, h : h + 1, :], (PROPS, length))
                for h in range(heads)
            ],
            axis=0,
        )
        valid = position < limit
        scores = jnp.where(valid, contract_last(query, k_ref[b]) - cum, masked_score)
        last = jnp.sum(jnp.where(position == limit - 1, cum, 0.0), axis=1, keepdims=True)
        prop_cum = last + contract_last(gate_pick, tree_gates[span], HIGHEST)
        live = jnp.concatenate([reached[span, span]] * heads, axis=0) * owner > 0.5
        tree = jnp.where(live, contract_last(query, new_k) - prop_cum, masked_score)
        top = jnp.maximum(
            jnp.max(scores, axis=1, keepdims=True), jnp.max(tree, axis=1, keepdims=True)
        )
        weights = jnp.where(valid, jnp.exp(scores - top), 0.0)
        tree_weights = jnp.where(live, jnp.exp(tree - top), 0.0)
        total = jnp.sum(weights, axis=1, keepdims=True) + jnp.sum(
            tree_weights, axis=1, keepdims=True
        )
        values = jnp.dot(weights.astype(bf16), v_ref[b], preferred_element_type=f32)
        values = values + jnp.dot(tree_weights.astype(bf16), new_v, preferred_element_type=f32)
        values = jnp.where(same_head, values, 0.0)
        t_hi, t_mid, t_low = split3(top)
        s_hi, s_mid, s_low = split3(total)
        part = lane // 16
        packed = jnp.where(
            part == 0,
            t_hi,
            jnp.where(
                part == 1, t_mid, jnp.where(part == 2, t_low, jnp.where(part == 3, s_hi, s_mid))
            ),
        )
        packed = jnp.where((lane % 16 == row_head) & (part < 5), packed, 0.0)
        picked_values = values[:PROPS]
        picked_packed = packed[:PROPS]
        for h in range(1, heads):
            picked_values = picked_values + values[h * PROPS : (h + 1) * PROPS]
            picked_packed = picked_packed + packed[h * PROPS : (h + 1) * PROPS]
        out_ref[span, :width] = picked_values.astype(bf16)
        out_ref[span, width:] = picked_packed.astype(bf16)

        start = pl.multiple_of(jnp.clip(limit, 0, length - window) // PROPS * PROPS, PROPS)
        select = start + iota((window, PROPS), 0) - limit == iota((window, PROPS), 1)
        select = jnp.where(select, 1.0, 0.0).astype(bf16)
        slot = start + iota((window, width), 0) - limit
        inside = (slot >= 0) & (slot < PROPS)
        for source, target, fresh in ((k_ref, ko_ref, new_k), (v_ref, vo_ref, new_v)):
            target[b] = source[b]
            placed = jnp.dot(select, fresh, preferred_element_type=f32)
            old = source[b, pl.ds(start, window), :].astype(f32)
            target[b, pl.ds(start, window), :] = jnp.where(inside, placed, old).astype(bf16)


def combine_kernel(
    n_kv,
    n_tp,
    heads,
    parts_ref,
    w_ref,
    out_ref,
    arrived,
    mine,
    gathered,
    partial,
    landed,
    send_a,
    recv_a,
    send_b,
    recv_b,
    send_c,
    recv_c,
):
    me = lax.axis_index("kv")
    tp = lax.axis_index("tp")
    width = heads * HEAD
    chunk_rows = parts_ref.shape[1]
    share = n_kv // n_tp
    barrier = pltpu.get_barrier_semaphore()
    for d in range(1, n_kv):
        pl.semaphore_signal(
            barrier, inc=1, device_id={"kv": lax.rem(me + d, n_kv)}, device_id_type=MESH
        )
    for d in range(1, n_tp):
        pl.semaphore_signal(
            barrier, inc=1, device_id={"tp": lax.rem(tp + d, n_tp)}, device_id_type=MESH
        )
    pl.semaphore_wait(barrier, n_kv - 1 + n_tp - 1)
    first = []
    for d in range(1, n_kv):
        peer = lax.rem(me + d, n_kv)
        copy = pltpu.make_async_remote_copy(
            src_ref=parts_ref.at[peer],
            dst_ref=arrived.at[d - 1],
            send_sem=send_a.at[d - 1],
            recv_sem=recv_a.at[d - 1],
            device_id={"kv": peer},
            device_id_type=MESH,
        )
        copy.start()
        first.append(copy)
    lane = iota((LANES, width), 0)
    fits = lane % 16 == iota((LANES, width), 1) // HEAD
    spread_top = jnp.where(fits & (lane < 48), 1.0, 0.0).astype(bf16)
    spread_sum = jnp.where(fits & (lane >= 48) & (lane < 80), 1.0, 0.0).astype(bf16)

    def unpack(block):
        packed = block[:, width:]
        return (
            jnp.dot(packed, spread_top, preferred_element_type=f32),
            jnp.dot(packed, spread_sum, preferred_element_type=f32),
            block[:, :width].astype(f32),
        )

    top, sums, values = unpack(parts_ref[me])
    for d in range(1, n_kv):
        first[d - 1].wait_recv()
        other_top, other_sums, other_values = unpack(arrived[d - 1])
        new_top = jnp.maximum(top, other_top)
        here, there = jnp.exp(top - new_top), jnp.exp(other_top - new_top)
        sums = here * sums + there * other_sums
        values = here * values + there * other_values
        top = new_top
    mine[...] = (values / sums).astype(bf16)
    second = []
    for d in range(1, n_kv):
        copy = pltpu.make_async_remote_copy(
            src_ref=mine,
            dst_ref=gathered.at[me],
            send_sem=send_b.at[d - 1],
            recv_sem=recv_b.at[d - 1],
            device_id={"kv": lax.rem(me + d, n_kv)},
            device_id_type=MESH,
        )
        copy.start()
        second.append(copy)
    gathered[me] = mine[...]
    for copy in second:
        copy.wait_recv()
    if chunk_rows % 16 == 0:
        attended = gathered[...].reshape(n_kv * chunk_rows, width)
        product = jnp.dot(attended, w_ref[...], preferred_element_type=f32).astype(bf16)
        partial[...] = product.reshape(partial.shape)
    else:

        def one(c, carry):
            partial[c] = jnp.dot(gathered[c], w_ref[...], preferred_element_type=f32).astype(bf16)
            return carry

        lax.fori_loop(0, n_kv, one, 0)
    third = []
    for d in range(1, n_tp):
        peer = lax.rem(tp + d, n_tp)
        copy = pltpu.make_async_remote_copy(
            src_ref=partial.at[pl.ds(peer * share, share)],
            dst_ref=landed.at[d - 1],
            send_sem=send_c.at[d - 1],
            recv_sem=recv_c.at[d - 1],
            device_id={"tp": peer},
            device_id_type=MESH,
        )
        copy.start()
        third.append(copy)
    total = partial[pl.ds(tp * share, share)].astype(f32)
    for d in range(1, n_tp):
        third[d - 1].wait_recv()
        total = total + landed[d - 1].astype(f32)
    out_ref[...] = total.astype(bf16)
    for copy in first + second + third:
        copy.wait_send()


def shards(
    n_kv,
    n_tp,
    tokens,
    norm_gain,
    w_query,
    w_key,
    w_value,
    w_gate,
    gate_bias,
    w_out,
    keys_cache,
    values_cache,
    cum_gates,
    prior_len,
    accepted,
    parents,
):
    row_count, depth = tokens.shape
    seq_count, length, width = keys_cache.shape
    heads = width // HEAD
    chunk_rows = row_count // n_kv
    columns = w_out.shape[1]
    vmem = pl.BlockSpec(memory_space=pltpu.VMEM)
    dma = pltpu.SemaphoreType.DMA
    proj_width = 3 * width + LANES
    out_width = width + LANES

    projected = pl.pallas_call(
        functools.partial(project_kernel, n_kv, heads),
        out_shape=jax.ShapeDtypeStruct((n_kv, chunk_rows, proj_width), bf16),
        in_specs=[vmem] * 7,
        out_specs=vmem,
        scratch_shapes=[
            pltpu.VMEM((2, n_kv // 2, chunk_rows, proj_width), bf16),
            pltpu.VMEM((n_kv // 2, chunk_rows, proj_width), bf16),
            pltpu.VMEM((n_kv // 2, chunk_rows, proj_width), bf16),
            pltpu.VMEM((n_kv // 2 - 1, chunk_rows, proj_width), bf16),
            pltpu.VMEM((2, n_kv // 2, chunk_rows, proj_width), bf16),
            pltpu.VMEM((chunk_rows, proj_width), bf16),
        ]
        + [dma((3,))] * 2
        + [dma((3 * (n_kv // 2 - 1),))] * 4
        + [dma((3,))] * 2,
        compiler_params=pltpu.CompilerParams(collective_id=0, has_side_effects=True),
        name="project",
    )(
        tokens.reshape(n_kv, chunk_rows, depth),
        norm_gain.reshape(1, depth),
        w_query,
        w_key,
        w_value,
        w_gate.T if depth % LANES == 0 else w_gate,
        gate_bias.reshape(1, -1),
    )
    projected = projected.reshape(row_count, proj_width)

    group = next(g for g in (4, 3, 2, 1) if seq_count % g == 0)
    rows = group * PROPS
    cache_spec = pl.BlockSpec((group, length, width), lambda s, *_: (s, 0, 0))
    keys_out, values_out, parts = pl.pallas_call(
        functools.partial(attend_kernel, heads),
        out_shape=(
            jax.ShapeDtypeStruct(keys_cache.shape, bf16),
            jax.ShapeDtypeStruct(values_cache.shape, bf16),
            jax.ShapeDtypeStruct((row_count, out_width), bf16),
        ),
        grid_spec=pltpu.PrefetchScalarGridSpec(
            num_scalar_prefetch=2,
            grid=(seq_count // group,),
            in_specs=[
                pl.BlockSpec((rows, proj_width), lambda s, *_: (s, 0)),
                pl.BlockSpec((PROPS, seq_count), lambda s, *_: (0, 0)),
                cache_spec,
                cache_spec,
                pl.BlockSpec((group, heads, length), lambda s, *_: (s, 0, 0)),
            ],
            out_specs=[
                cache_spec,
                cache_spec,
                pl.BlockSpec((rows, out_width), lambda s, *_: (s, 0)),
            ],
        ),
        name="attend",
    )(
        prior_len,
        accepted,
        projected,
        parents.T,
        keys_cache,
        values_cache,
        cum_gates,
    )

    mixed = pl.pallas_call(
        functools.partial(combine_kernel, n_kv, n_tp, heads),
        out_shape=jax.ShapeDtypeStruct((n_kv // n_tp, chunk_rows, columns), bf16),
        in_specs=[vmem] * 2,
        out_specs=vmem,
        scratch_shapes=[
            pltpu.VMEM((n_kv - 1, chunk_rows, out_width), bf16),
            pltpu.VMEM((chunk_rows, width), bf16),
            pltpu.VMEM((n_kv, chunk_rows, width), bf16),
            pltpu.VMEM((n_kv, chunk_rows, columns), bf16),
            pltpu.VMEM((n_tp - 1, n_kv // n_tp, chunk_rows, columns), bf16),
        ]
        + [dma((n_kv - 1,))] * 4
        + [dma((n_tp - 1,))] * 2,
        compiler_params=pltpu.CompilerParams(collective_id=1, has_side_effects=True),
        name="combine",
    )(parts.reshape(n_kv, chunk_rows, out_width), w_out)
    return (mixed.reshape(row_count // n_tp, columns), keys_out, values_out)


def solution(mesh):
    placed = (
        P(None, "kv"),
        P("kv"),
        P("kv", "tp"),
        P("kv", "tp"),
        P("kv", "tp"),
        P(),
        P(),
        P("tp", "kv"),
        P(None, "kv", "tp"),
        P(None, "kv", "tp"),
        P(None, "tp", "kv"),
        P(),
        P(),
        P(),
    )
    return jax.shard_map(
        functools.partial(shards, mesh.shape["kv"], mesh.shape["tp"]),
        mesh=mesh,
        in_specs=placed,
        out_specs=(P("tp", "kv"), P(None, "kv", "tp"), P(None, "kv", "tp")),
        check_vma=False,
    )
```

profile of v0, /device:TPU:0, one launch (start us, length us, event | category | flops | bytes accessed | tf_op | source)
XLA Modules:
  0.0 79.2 jit_solution(13368057750281725534)
XLA Ops:
  0.6 33.5 %project.1 = bf16[8,48,896]{2,1,0:T(8,128)(2,1)} custom-call(bf16[8,48,256]{2,1,0:T(8,128)(2,1)} %bitcast.11, f32[1,256]{1,0:T(1,128)} %bitcast.14, bf16[256,256]{1,0:T(8,128)(2,1)} %wq_ref.1, bf16[256,256]{1,0:T(8,128)(2,1)} %wk_ref.1, bf16[256,256]{1,0:T(8,128)(2,1)} %wv_ref.1, bf16[16,2048]{1,0:T(8,128)(2,1)} %bitcast.12, f32[1,16]{1,0:T(1,128)} %bitcast.15), custom_call_target="tpu_custom_call" | custom-call | tf_op jit(solution)/shard_map/project/pallas_call | solution.py:456
  34.1 20.9 %attend.1 = (bf16[24,512,256]{2,1,0:T(8,128)(2,1)}, bf16[24,512,256]{2,1,0:T(8,128)(2,1)}, bf16[384,384]{1,0:T(8,128)(2,1)}) custom-call(s32[24]{0:T(128)} %prior_s.1, s32[24]{0:T(128)} %accepted_s.1, bf16[384,896]{1,0:T(8,128)(2,1)} %bitcast.8, s32[16,24]{1,0:T(8,128)} %bitcast.13, bf16[24,512,256]{2,1,0:T(8,128)(2,1)} %k_ref.1, ...), custom_call_target="tpu_custom_call" | custom-call | tf_op jit(solution)/shard_map/attend/pallas_call | solution.py:488
  55.0 22.7 %combine.1 = bf16[2,48,256]{2,1,0:T(8,128)(2,1)} custom-call(bf16[8,48,384]{2,1,0:T(8,128)(2,1)} %bitcast.9, bf16[256,256]{1,0:T(8,128)(2,1)} %w_ref.1), custom_call_target="tpu_custom_call" | custom-call | tf_op jit(solution)/shard_map/combine/pallas_call | solution.py:522
  77.8 1.4 %copy.18 = bf16[96,256]{1,0:T(8,128)(2,1)} copy(bf16[96,256]{1,0:T(8,128)(2,1)} %bitcast.10) | data formatting | bytes 98304
where the time goes:
time: 79.4 us; the launch traced here: 79.2 us
  Pallas kernels  77.1 us (97%)
  local copies, waits for them, and re-layouts  1.42 us (2%)
    pallas_call x1, Pallas kernels, shards(): pl.pallas_call(functools.partial(project_kernel, n_kv, heads), out_shape=...  33.5 us
    pallas_call x1, Pallas kernels, shards(): pl.pallas_call(functools.partial(combine_kernel, n_kv, n_tp, heads), out_...  22.7 us
    pallas_call x1, Pallas kernels, shards(): pl.pallas_call(functools.partial(attend_kernel, heads), out_shape=(jax.Sh...  20.9 us

commit v1 on v0

v1 whole, which is shorter than its diff:
```python
import functools

import jax
import jax.numpy as jnp
from jax import lax
from jax.experimental import pallas as pl
from jax.experimental.pallas import tpu as pltpu
from jax.sharding import PartitionSpec as P

HEAD = 64
PROPS = 16
LANES = 128
SQUARE_ROW = 7
SUM_ROW = 4
masked_score = -1e30
norm_eps = 1e-06
MESH = pl.DeviceIdType.MESH
f32, bf16, i32 = jnp.float32, jnp.bfloat16, jnp.int32


def iota(shape, axis):
    return lax.broadcasted_iota(i32, shape, axis)


def ones_where(mask, dtype=f32):
    return jnp.where(mask, 1.0, 0.0).astype(dtype)


def split2(x):
    hi = x.astype(bf16)
    return hi, (x - hi.astype(f32)).astype(bf16)


def split3(x):
    hi = x.astype(bf16).astype(f32)
    mid = (x - hi).astype(bf16).astype(f32)
    return hi, mid, x - hi - mid


def contract_last(a, b):
    return lax.dot_general(a, b, (((1,), (1,)), ((), ())), preferred_element_type=f32)


def matmul(a, b):
    return jnp.dot(a, b, preferred_element_type=f32)


def step_kernel(
    n_kv,
    n_tp,
    heads,
    per,
    prior_s,
    accepted_s,
    tokens_ref,
    gain_ref,
    wq_ref,
    wk_ref,
    wv_ref,
    wg_ref,
    bias_ref,
    wout_ref,
    parents_ref,
    k_hbm,
    v_hbm,
    cum_hbm,
    mixed_ref,
    newk_ref,
    newv_ref,
    kbuf,
    vbuf,
    cumbuf,
    part,
    gpart,
    arr1,
    garr1,
    half,
    ghalf,
    arr2,
    garr2,
    full,
    gfull,
    wall,
    parts_v,
    parts_s,
    got_v,
    got_s,
    mine,
    att,
    load_sems,
    s1_send,
    s1_recv,
    s2_send,
    s2_recv,
    s3_send,
    s3_recv,
    w_send,
    w_recv,
    cv_send,
    cv_recv,
    cs_send,
    cs_recv,
    ag_send,
    ag_recv,
):
    me = lax.axis_index("kv")
    tp = lax.axis_index("tp")
    n_chunks, rc, depth = tokens_ref.shape
    length = kbuf.shape[1]
    width = heads * HEAD
    lines = heads * PROPS
    cq = n_chunks // 4
    n_groups = n_kv // 4
    cpt = n_chunks // n_tp
    corner, group = lax.rem(me, 4), me // 4
    quarter = pl.ds(corner * cq, cq)

    barrier = pltpu.get_barrier_semaphore()
    for d in range(1, n_kv * n_tp):
        other = lax.rem(me * n_tp + tp + d, n_kv * n_tp)
        pl.semaphore_signal(
            barrier,
            inc=1,
            device_id={"kv": other // n_tp, "tp": lax.rem(other, n_tp)},
            device_id_type=MESH,
        )
    loads = []
    for c in range(n_chunks):
        span = pl.ds(c * per, per)
        for at, (source, target) in enumerate(((k_hbm, kbuf), (v_hbm, vbuf), (cum_hbm, cumbuf))):
            copy = pltpu.make_async_copy(source.at[span], target.at[span], load_sems.at[at, c])
            copy.start()
            loads.append(copy)

    def send(source, target, sems, at, kv=None, to_tp=None):
        where = {}
        if kv is not None:
            where["kv"] = kv
        if to_tp is not None:
            where["tp"] = to_tp
        copy = pltpu.make_async_remote_copy(
            src_ref=source,
            dst_ref=target,
            send_sem=sems[0].at[at],
            recv_sem=sems[1].at[at],
            device_id=where,
            device_id_type=MESH,
        )
        copy.start()
        return copy

    total_heads = bias_ref.shape[1]
    pick = (iota((8, total_heads), 1) == tp * heads + iota((8, total_heads), 0)) & (
        iota((8, total_heads), 0) < heads
    )
    if depth % LANES == 0:
        gate_w = wg_ref[:, pl.ds(pl.multiple_of(me * depth, depth), depth)]
        gate_w = matmul(ones_where(pick, bf16), gate_w).astype(bf16)
    else:
        gate_w = wg_ref[pl.ds(pl.multiple_of(me * depth, depth), depth), :]
        gate_w = contract_last(ones_where(pick, bf16), gate_w).astype(bf16)
    square_w = ones_where(iota((8, depth), 0) == SQUARE_ROW, bf16)
    floats = tokens_ref[...].reshape(n_chunks * rc, depth).astype(f32)
    scaled = (floats * gain_ref[...]).astype(bf16)

    def product(piece, w_ref):
        value = matmul(scaled, w_ref[...]).astype(bf16)
        part[piece] = value.reshape(n_chunks, rc, width)

    product(0, wq_ref)
    sq_hi, sq_lo = split2(floats * floats)
    gpart[...] = jnp.zeros_like(gpart)
    for c in range(n_chunks):
        rows = slice(c * rc, (c + 1) * rc)
        gpart[c, :, :rc] = (
            contract_last(gate_w, scaled[rows])
            + contract_last(square_w, sq_hi[rows])
            + contract_last(square_w, sq_lo[rows])
        )

    pl.semaphore_wait(barrier, n_kv * n_tp - 1)
    started = []

    def corner_sends(sources, targets, sems, piece):
        out = []
        for d in range(1, 4):
            there = lax.rem(corner + d, 4)
            out.append(
                send(
                    sources(there), targets(d), sems, piece * 3 + d - 1, kv=group * 4 + there
                )
            )
        started.extend(out)
        return out

    def first_stage(piece):
        return corner_sends(
            lambda there: part.at[piece, pl.ds(there * cq, cq)],
            lambda d: arr1.at[piece, d - 1],
            (s1_send, s1_recv),
            piece,
        )

    def group_sends(source, target, piece):
        out = []
        for d in range(1, n_groups):
            there = lax.rem(group + d, n_groups) * 4 + corner
            out.append(
                send(
                    source,
                    target(d),
                    (s2_send, s2_recv),
                    piece * (n_groups - 1) + d - 1,
                    kv=there,
                )
            )
        started.extend(out)
        return out

    def second_stage(piece, stage):
        for copy in stage:
            copy.wait_recv()
        total = part[piece, quarter].astype(f32)
        for d in range(3):
            total = total + arr1[piece, d].astype(f32)
        half[piece] = total.astype(bf16)
        return group_sends(half.at[piece], lambda d: arr2.at[piece, d - 1], piece)

    def third_stage(piece, stage, columns):
        for copy in stage:
            copy.wait_recv()
        total = half[piece].astype(f32)
        for d in range(n_groups - 1):
            total = total + arr2[piece, d].astype(f32)
        for j in range(cq):
            full[piece, corner * cq + j] = (total[j] * columns[j]).astype(bf16)
        return corner_sends(
            lambda there: full.at[piece, quarter],
            lambda d: full.at[piece, quarter],
            (s3_send, s3_recv),
            piece,
        )

    q1 = first_stage(0)
    g1 = corner_sends(
        lambda there: gpart.at[pl.ds(there * cq, cq)],
        lambda d: garr1.at[d - 1],
        (s1_send, s1_recv),
        3,
    )
    product(1, wk_ref)
    k1 = first_stage(1)
    product(2, wv_ref)

    slot = lax.rem(me, n_tp) * cpt + me // n_tp
    own = jnp.minimum(slot, n_chunks - 1)
    every = parents_ref[...]
    parent = jnp.concatenate(
        [
            jnp.sum(
                jnp.where(iota(every.shape, 1) == own * per + k, every, 0).astype(f32),
                axis=1,
                keepdims=True,
            ).astype(i32)
            for k in range(per)
        ],
        axis=0,
    )
    row, column = iota((rc, rc), 0), iota((rc, rc), 1)
    link = (parent + (row // PROPS) * PROPS == column) & (parent >= 0)
    reached = ones_where(link | (row == column))
    for squaring in range((PROPS - 1).bit_length()):
        reached = jnp.minimum(matmul(reached.astype(bf16), reached.astype(bf16)), 1.0)

    q2 = second_stage(0, q1)
    for copy in g1:
        copy.wait_recv()
    ghalf[...] = gpart[quarter] + garr1[0] + garr1[1] + garr1[2]
    g2 = group_sends(ghalf, lambda d: garr2.at[d - 1], 3)
    v1 = first_stage(2)
    w_copies = []
    for d in range(1, n_tp):
        w_copies.append(
            send(
                wout_ref, wall.at[tp], (w_send, w_recv), d - 1, to_tp=lax.rem(tp + d, n_tp)
            )
        )
    started.extend(w_copies)
    wall[tp] = wout_ref[...]

    for copy in g2:
        copy.wait_recv()
    gates = ghalf[...]
    for d in range(n_groups - 1):
        gates = gates + garr2[d]
    bias = jnp.sum(
        jnp.where(pick, jnp.broadcast_to(bias_ref[...], (8, total_heads)), 0.0),
        axis=1,
        keepdims=True,
    )
    inv_columns = []
    eye = iota((rc, LANES), 0) == iota((rc, LANES), 1)
    for j in range(cq):
        inv_row = lax.rsqrt(
            gates[j, SQUARE_ROW : SQUARE_ROW + 1, :] / (n_kv * depth) + norm_eps
        )
        pre = inv_row * gates[j] + bias
        gfull[corner * cq + j] = jnp.minimum(pre, 0.0) - jnp.log1p(jnp.exp(-jnp.abs(pre)))
        inv_columns.append(
            jnp.sum(
                jnp.where(eye, jnp.broadcast_to(inv_row, (rc, LANES)), 0.0),
                axis=1,
                keepdims=True,
            )
        )
    q3 = third_stage(0, q2, [c * HEAD ** (-0.5) for c in inv_columns])
    g3 = corner_sends(
        lambda there: gfull.at[quarter], lambda d: gfull.at[quarter], (s3_send, s3_recv), 3
    )
    k2 = second_stage(1, k1)
    v2 = second_stage(2, v1)

    lane_head = iota((PROPS, width), 1) // HEAD
    head_rows = [ones_where(lane_head == h) for h in range(heads)]
    head_mask = jnp.concatenate(head_rows, axis=0).astype(bf16)
    position = iota((lines, length), 1)
    short_position = iota((heads, length), 1)
    line_eye = iota((lines, LANES), 0) == iota((lines, LANES), 1)
    last_lane = iota((heads, LANES), 1) - LANES // 2
    last_mask = (last_lane >= 0) & (last_lane // PROPS == iota((heads, LANES), 0))
    tile_row = iota((8, LANES), 0)
    offset = me * length

    def as_row(value):
        return jnp.sum(jnp.where(line_eye, value, 0.0), axis=0, keepdims=True)

    def attend(owner):
        chunk = jnp.minimum(lax.rem(owner, n_tp) * cpt + owner // n_tp, n_chunks - 1)
        limits, scores = [], []
        for k in range(per):
            seq = chunk * per + k
            limits.append(prior_s[seq] + accepted_s[seq] - offset)
            query = full[0, chunk, k * PROPS : (k + 1) * PROPS, :]
            query = jnp.concatenate([query] * heads, axis=0) * head_mask
            scores.append(contract_last(query, kbuf[seq]))
        tile = jnp.zeros((8, LANES), f32)
        weights = []
        for k in range(per):
            seq = chunk * per + k
            cum = jnp.concatenate(
                [
                    jnp.broadcast_to(cumbuf[seq, h : h + 1, :], (PROPS, length))
                    for h in range(heads)
                ],
                axis=0,
            )
            value = jnp.where(position < limits[k], scores[k] - cum, masked_score)
            top = jnp.max(value, axis=1, keepdims=True)
            weight = jnp.exp(value - top)
            total = jnp.sum(weight, axis=1, keepdims=True)
            weights.append(weight.astype(bf16))
            last = jnp.sum(
                jnp.where(short_position == limits[k] - 1, cumbuf[seq], 0.0),
                axis=1,
                keepdims=True,
            )
            last_row = jnp.sum(jnp.where(last_mask, last, 0.0), axis=0, keepdims=True)
            tile = jnp.where(tile_row == k, as_row(top) + last_row, tile)
            tile = jnp.where(tile_row == SUM_ROW + k, as_row(total), tile)
        for k in range(per):
            values = matmul(weights[k], vbuf[chunk * per + k])
            picked = values[:PROPS] * head_rows[0]
            for h in range(1, heads):
                picked = picked + values[h * PROPS : (h + 1) * PROPS] * head_rows[h]
            parts_v[owner, k * PROPS : (k + 1) * PROPS, :] = picked.astype(bf16)
        parts_s[owner] = tile

    def part_copies(d):
        owner = lax.rem(me + d, n_kv)
        return [
            pltpu.make_async_remote_copy(
                src_ref=source.at[owner],
                dst_ref=target.at[d - 1],
                send_sem=send_sem.at[d - 1],
                recv_sem=recv_sem.at[d - 1],
                device_id={"kv": owner},
                device_id_type=MESH,
            )
            for source, target, send_sem, recv_sem in (
                (parts_v, got_v, cv_send, cv_recv),
                (parts_s, got_s, cs_send, cs_recv),
            )
        ]

    def attend_and_send(d):
        attend(lax.rem(me + d, n_kv))
        for copy in part_copies(d):
            copy.start()

    for copy in loads:
        copy.wait()
    for copy in q3:
        copy.wait_recv()
    attend_and_send(1)
    k3 = third_stage(1, k2, inv_columns)
    attend_and_send(2)
    v3 = third_stage(2, v2, inv_columns)

    def one(d, carry):
        attend_and_send(d)
        return carry

    lax.fori_loop(3, n_kv, one, 0)
    attend(me)

    for copy in g3 + k3:
        copy.wait_recv()
    gate_parts = jnp.concatenate(split3(gfull[own]), axis=0)[:, :rc].astype(bf16)
    tree_gates = contract_last(gate_parts, reached.astype(bf16))
    tree_gates = tree_gates[0:8] + tree_gates[8:16] + tree_gates[16:24]
    wide_rows = [ones_where(iota((rc, width), 1) // HEAD == h) for h in range(heads)]
    wide_mask = jnp.concatenate(wide_rows, axis=0).astype(bf16)
    tree_query = jnp.concatenate([full[0, own]] * heads, axis=0) * wide_mask
    tree = contract_last(tree_query, full[1, own])
    tree = tree - jnp.concatenate(
        [jnp.broadcast_to(tree_gates[h : h + 1, :], (rc, rc)) for h in range(heads)], axis=0
    )
    live = jnp.concatenate([reached] * heads, axis=0) > 0.5
    tree = jnp.where(live, tree, masked_score)
    tree_top = jnp.max(tree, axis=1, keepdims=True)
    tree_weights = jnp.where(live, jnp.exp(tree - tree_top), 0.0)
    tree_sum = jnp.sum(tree_weights, axis=1, keepdims=True)
    for copy in v3:
        copy.wait_recv()
    tree_values = matmul(tree_weights.astype(bf16), full[2, own])
    tree_picked = tree_values[:rc] * wide_rows[0]
    for h in range(1, heads):
        tree_picked = tree_picked + tree_values[h * rc : (h + 1) * rc] * wide_rows[h]
    newk_ref[...] = full[1]
    newv_ref[...] = full[2]

    def tile_of(value):
        rows = [
            as_row(
                jnp.concatenate(
                    [
                        value[h * rc + k * PROPS : h * rc + (k + 1) * PROPS]
                        for h in range(heads)
                    ],
                    axis=0,
                )
            )
            for k in range(per)
        ]
        rows = rows + [jnp.zeros((1, LANES), f32)] * (4 - per)
        return jnp.concatenate(rows, axis=0)

    tree_top_tile, tree_sum_tile = tile_of(tree_top), tile_of(tree_sum)

    landing = [part_copies(d) for d in range(1, n_kv)]
    for pair in landing:
        pair[1].wait_recv()
    tiles = [parts_s[me]] + [got_s[d] for d in range(n_kv - 1)]
    last = tiles[0][:4]
    for tile in tiles[1:]:
        last = last + tile[:4]
    last = pltpu.roll(last, LANES // 2, axis=1)
    lane_ok = iota((4, LANES), 1) < lines
    tops = [jnp.where(lane_ok, tile[:4], 0.0) for tile in tiles]
    tops.append(jnp.where(lane_ok, tree_top_tile - last, 0.0))
    sums = [jnp.where(lane_ok, tile[4:], 1.0) for tile in tiles] + [
        jnp.where(lane_ok, tree_sum_tile, 1.0)
    ]
    top = functools.reduce(jnp.maximum, tops)
    scales = [jnp.exp(t - top) for t in tops]
    total = functools.reduce(lambda a, b: a + b, [a * b for a, b in zip(scales, sums)])
    spread = ones_where(
        (iota((LANES, width), 0) // PROPS == iota((LANES, width), 1) // HEAD)
        & (iota((LANES, width), 0) < lines),
        bf16,
    )
    fits = (iota((PROPS, LANES), 1) % PROPS == iota((PROPS, LANES), 0)) & (
        iota((PROPS, LANES), 1) < lines
    )

    def expand(scale):
        scale = scale / total
        rows = jnp.concatenate(
            [
                jnp.where(fits, jnp.broadcast_to(scale[k : k + 1], (PROPS, LANES)), 0.0)
                for k in range(per)
            ],
            axis=0,
        )
        hi, lo = split2(rows)
        return matmul(hi, spread) + matmul(lo, spread)

    result = expand(scales[-1]) * tree_picked
    result = result + expand(scales[0]) * parts_v[me].astype(f32)
    for d in range(n_kv - 1):
        landing[d][0].wait_recv()
        result = result + expand(scales[d + 1]) * got_v[d].astype(f32)
    mine[...] = result.astype(bf16)

    target, early = lax.rem(me, n_tp), me // n_tp
    spreads = [
        pltpu.make_async_remote_copy(
            src_ref=mine,
            dst_ref=att.at[jnp.minimum(early, cpt - 1), tp],
            send_sem=ag_send.at[d],
            recv_sem=ag_recv.at[jnp.minimum(early, cpt - 1) * n_tp + tp],
            device_id={"kv": lax.rem(me + d, n_kv), "tp": target},
            device_id_type=MESH,
        )
        for d in range(n_kv)
    ]
    sends = early < cpt
    for d in range(1, n_kv):

        @pl.when(sends)
        def _(d=d):
            spreads[d].start()

    @pl.when(sends & (target != tp))
    def _():
        spreads[0].start()

    @pl.when(sends & (target == tp))
    def _():
        att[jnp.minimum(early, cpt - 1), tp] = mine[...]

    for copy in w_copies:
        copy.wait_recv()
    for at in range(cpt * n_tp):
        e, t = at // n_tp, at % n_tp

        @pl.when((me != e * n_tp + tp) | (tp != t))
        def _(at=at, e=e, t=t):
            pltpu.make_async_remote_copy(
                src_ref=mine,
                dst_ref=att.at[e, t],
                send_sem=ag_send.at[0],
                recv_sem=ag_recv.at[at],
                device_id={"kv": me, "tp": lax.rem(tp + 1, n_tp)},
                device_id_type=MESH,
            ).wait_recv()

    mixed = None
    for t in range(n_tp):
        rows = jnp.concatenate([att[e, t] for e in range(cpt)], axis=0)
        piece = matmul(rows, wall[t]).astype(bf16).astype(f32)
        mixed = piece if mixed is None else mixed + piece
    mixed_ref[...] = mixed.astype(bf16)

    for d in range(1, n_kv):

        @pl.when(sends)
        def _(d=d):
            spreads[d].wait_send()

    @pl.when(sends & (target != tp))
    def _():
        spreads[0].wait_send()

    for copy in started:
        copy.wait_send()
    for pair in landing:
        for copy in pair:
            copy.wait_send()


def write_kernel(
    prior_s,
    accepted_s,
    newk_ref,
    newv_ref,
    mixed_in,
    k_ref,
    v_ref,
    mixed_ref,
    ko_ref,
    vo_ref,
    windows,
    bulk_sems,
    window_sems,
):
    seq_count, length, width = k_ref.shape
    window = 2 * PROPS
    offset = lax.axis_index("kv") * length
    bulk = []
    for b in range(seq_count):
        for at, (source, target) in enumerate(((k_ref, ko_ref), (v_ref, vo_ref))):
            copy = pltpu.make_async_copy(source.at[b], target.at[b], bulk_sems.at[at, b])
            copy.start()
            bulk.append(copy)
    mixed_ref[...] = mixed_in[...]
    placed = []
    for b in range(seq_count):
        limit = prior_s[b] + accepted_s[b] - offset
        start = pl.multiple_of(jnp.clip(limit, 0, length - window) // PROPS * PROPS, PROPS)
        select = start + iota((window, PROPS), 0) - limit == iota((window, PROPS), 1)
        select = ones_where(select, bf16)
        slot = start + iota((window, width), 0) - limit
        inside = (slot >= 0) & (slot < PROPS)
        for at, (source, fresh, target) in enumerate(
            ((k_ref, newk_ref, ko_ref), (v_ref, newv_ref, vo_ref))
        ):
            rows = matmul(select, fresh[b * PROPS : (b + 1) * PROPS])
            old = source[b, pl.ds(start, window), :].astype(f32)
            windows[at, b] = jnp.where(inside, rows, old).astype(bf16)
            placed.append(
                pltpu.make_async_copy(
                    windows.at[at, b],
                    target.at[b, pl.ds(start, window), :],
                    window_sems.at[at, b],
                )
            )
    for first, second in zip(bulk, placed):
        first.wait()
        second.start()
    for copy in placed:
        copy.wait()


def shards(
    n_kv,
    n_tp,
    tokens,
    norm_gain,
    w_query,
    w_key,
    w_value,
    w_gate,
    gate_bias,
    w_out,
    keys_cache,
    values_cache,
    cum_gates,
    prior_len,
    accepted,
    parents,
):
    row_count, depth = tokens.shape
    seq_count, length, width = keys_cache.shape
    heads = width // HEAD
    per = next(p for p in range(1, 5) if seq_count % p == 0 and seq_count // p <= n_kv)
    n_chunks = seq_count // per
    rc = per * PROPS
    cq = n_chunks // 4
    n_groups = n_kv // 4
    cpt = n_chunks // n_tp
    columns = w_out.shape[1]
    vmem = pl.BlockSpec(memory_space=pltpu.VMEM)
    smem = pl.BlockSpec(memory_space=pltpu.SMEM)
    hbm = pl.BlockSpec(memory_space=pltpu.HBM)
    dma = pltpu.SemaphoreType.DMA

    mixed, new_keys, new_values = pl.pallas_call(
        functools.partial(step_kernel, n_kv, n_tp, heads, per),
        out_shape=(
            jax.ShapeDtypeStruct((cpt * rc, columns), bf16),
            jax.ShapeDtypeStruct((n_chunks, rc, width), bf16),
            jax.ShapeDtypeStruct((n_chunks, rc, width), bf16),
        ),
        in_specs=[smem] * 2 + [vmem] * 9 + [hbm] * 3,
        out_specs=[vmem] * 3,
        scratch_shapes=[
            pltpu.VMEM((seq_count, length, width), bf16),
            pltpu.VMEM((seq_count, length, width), bf16),
            pltpu.VMEM((seq_count, heads, length), f32),
            pltpu.VMEM((3, n_chunks, rc, width), bf16),
            pltpu.VMEM((n_chunks, 8, LANES), f32),
            pltpu.VMEM((3, 3, cq, rc, width), bf16),
            pltpu.VMEM((3, cq, 8, LANES), f32),
            pltpu.VMEM((3, cq, rc, width), bf16),
            pltpu.VMEM((cq, 8, LANES), f32),
            pltpu.VMEM((3, n_groups - 1, cq, rc, width), bf16),
            pltpu.VMEM((n_groups - 1, cq, 8, LANES), f32),
            pltpu.VMEM((3, n_chunks, rc, width), bf16),
            pltpu.VMEM((n_chunks, 8, LANES), f32),
            pltpu.VMEM((n_tp, width, columns), bf16),
            pltpu.VMEM((n_kv, rc, width), bf16),
            pltpu.VMEM((n_kv, 8, LANES), f32),
            pltpu.VMEM((n_kv - 1, rc, width), bf16),
            pltpu.VMEM((n_kv - 1, 8, LANES), f32),
            pltpu.VMEM((rc, width), bf16),
            pltpu.VMEM((cpt, n_tp, rc, width), bf16),
            dma((3, n_chunks)),
            dma((12,)),
            dma((12,)),
            dma((4 * (n_groups - 1),)),
            dma((4 * (n_groups - 1),)),
            dma((12,)),
            dma((12,)),
            dma((n_tp - 1,)),
            dma((n_tp - 1,)),
            dma((n_kv - 1,)),
            dma((n_kv - 1,)),
            dma((n_kv - 1,)),
            dma((n_kv - 1,)),
            dma((n_kv,)),
            dma((cpt * n_tp,)),
        ],
        compiler_params=pltpu.CompilerParams(
            collective_id=0, has_side_effects=True, vmem_limit_bytes=28 * 1024 * 1024
        ),
        name="step",
    )(
        prior_len,
        accepted,
        tokens.reshape(n_chunks, rc, depth),
        norm_gain.reshape(1, depth),
        w_query,
        w_key,
        w_value,
        w_gate.T if depth % LANES == 0 else w_gate,
        gate_bias.reshape(1, -1),
        w_out,
        parents.T,
        keys_cache,
        values_cache,
        cum_gates,
    )

    return pl.pallas_call(
        write_kernel,
        out_shape=(
            jax.ShapeDtypeStruct((cpt * rc, columns), bf16),
            jax.ShapeDtypeStruct(keys_cache.shape, bf16),
            jax.ShapeDtypeStruct(values_cache.shape, bf16),
        ),
        in_specs=[smem] * 2 + [vmem] * 5,
        out_specs=[vmem, hbm, hbm],
        scratch_shapes=[
            pltpu.VMEM((2, seq_count, 2 * PROPS, width), bf16),
            dma((2, seq_count)),
            dma((2, seq_count)),
        ],
        name="write",
    )(
        prior_len,
        accepted,
        new_keys.reshape(row_count, width),
        new_values.reshape(row_count, width),
        mixed,
        keys_cache,
        values_cache,
    )


def solution(mesh):
    placed = (
        P(None, "kv"),
        P("kv"),
        P("kv", "tp"),
        P("kv", "tp"),
        P("kv", "tp"),
        P(),
        P(),
        P("tp", "kv"),
        P(None, "kv", "tp"),
        P(None, "kv", "tp"),
        P(None, "tp", "kv"),
        P(),
        P(),
        P(),
    )
    return jax.shard_map(
        functools.partial(shards, mesh.shape["kv"], mesh.shape["tp"]),
        mesh=mesh,
        in_specs=placed,
        out_specs=(P("tp", "kv"), P(None, "kv", "tp"), P(None, "kv", "tp")),
        check_vma=False,
    )
```

time: 79.4 us -> 67.2 us (0.85)
  the two profiles are of different devices: /device:TPU:0 before, /device:TPU:5 now
where the time goes in v1:
time: 67.2 us; the launch traced here: 66.8 us
  Pallas kernels  48.9 us (73%)
  local copies, waits for them, and re-layouts  17.2 us (26%)
    pallas_call x1, Pallas kernels, shards(): pl.pallas_call(functools.partial(step_kernel, n_kv, n_tp, heads, per), ou...  37.4 us
    unnamed x34, local copies, waits for them, and re-layouts  17.2 us
    pallas_call x1, Pallas kernels, shards(): pl.pallas_call(write_kernel, out_shape=(jax.ShapeDtypeStruct((cpt * rc, c...  11.6 us

profile of v1, /device:TPU:5, one launch (start us, length us, event | category | flops | bytes accessed | tf_op | source)
XLA Modules:
  0.0 66.8 jit_solution(11646140856961819933)
XLA Ops:
  0.6 0.0 copy-start
  0.6 2.8 %copy-done = bf16[24,512,256]{2,1,0:T(8,128)(2,1)S(1)} copy-done((bf16[24,512,256]{2,1,0:T(8,128)(2,1)S(1)}, bf16[24,512,256]{2,1,0:T(8,128)(2,1)}, u32[]{:S(2)}) %copy-start) | copy-done | bytes 6291480
  3.4 0.0 copy-start.1
  3.4 2.8 %copy-done.1 = bf16[24,512,256]{2,1,0:T(8,128)(2,1)S(1)} copy-done((bf16[24,512,256]{2,1,0:T(8,128)(2,1)S(1)}, bf16[24,512,256]{2,1,0:T(8,128)(2,1)}, u32[]{:S(2)}) %copy-start.1) | copy-done | bytes 6291480
  6.2 0.0 copy-start.2
  6.2 0.9 %copy-done.2 = bf16[384,256]{1,0:T(8,128)(2,1)S(1)} copy-done((bf16[384,256]{1,0:T(8,128)(2,1)S(1)}, bf16[384,256]{1,0:T(8,128)(2,1)}, u32[]{:S(2)}) %copy-start.2) | copy-done | bytes 196632
  7.1 0.0 copy-start.3
  7.1 0.9 %copy-done.3 = f32[24,4,512]{2,1,0:T(4,128)S(1)} copy-done((f32[24,4,512]{2,1,0:T(4,128)S(1)}, f32[24,4,512]{2,1,0:T(4,128)}, u32[]{:S(2)}) %copy-start.3) | copy-done | bytes 196632
  8.1 0.0 copy-start.6
  8.1 0.9 %copy-done.6 = bf16[256,256]{1,0:T(8,128)(2,1)S(1)} copy-done((bf16[256,256]{1,0:T(8,128)(2,1)S(1)}, bf16[256,256]{1,0:T(8,128)(2,1)}, u32[]{:S(2)}) %copy-start.6) | copy-done | bytes 131096
  9.0 0.0 copy-start.7
  9.0 0.9 %copy-done.7 = bf16[256,256]{1,0:T(8,128)(2,1)S(1)} copy-done((bf16[256,256]{1,0:T(8,128)(2,1)S(1)}, bf16[256,256]{1,0:T(8,128)(2,1)}, u32[]{:S(2)}) %copy-start.7) | copy-done | bytes 131096
  9.9 0.0 copy-start.8
  9.9 0.9 %copy-done.8 = bf16[256,256]{1,0:T(8,128)(2,1)S(1)} copy-done((bf16[256,256]{1,0:T(8,128)(2,1)S(1)}, bf16[256,256]{1,0:T(8,128)(2,1)}, u32[]{:S(2)}) %copy-start.8) | copy-done | bytes 131096
  10.8 0.0 copy-start.9
  10.8 0.9 %copy-done.9 = bf16[256,256]{1,0:T(8,128)(2,1)S(1)} copy-done((bf16[256,256]{1,0:T(8,128)(2,1)S(1)}, bf16[256,256]{1,0:T(8,128)(2,1)}, u32[]{:S(2)}) %copy-start.9) | copy-done | bytes 131096
  11.7 0.0 copy-start.10
  11.7 0.8 %copy-done.10 = bf16[2048,16]{0,1:T(8,128)(2,1)S(1)} copy-done((bf16[2048,16]{0,1:T(8,128)(2,1)S(1)}, bf16[2048,16]{0,1:T(8,128)(2,1)}, u32[]{:S(2)}) %copy-start.10) | copy-done | bytes 65560
  12.5 0.0 copy-start.12
  12.5 0.7 %copy-done.12 = s32[24,16]{0,1:T(8,128)S(1)} copy-done((s32[24,16]{0,1:T(8,128)S(1)}, s32[24,16]{0,1:T(8,128)}, u32[]{:S(2)}) %copy-start.12) | copy-done | bytes 1560
  13.2 0.0 copy-start.13
  13.2 0.7 copy-done.13
  13.9 0.0 copy-start.14
  13.9 0.7 copy-done.14
  14.5 0.7 %copy-done.15 = f32[256]{0:T(256)S(1)} copy-done((f32[256]{0:T(256)S(1)}, f32[256]{0:T(256)}, u32[]{:S(2)}) %copy-start.15) | copy-done | bytes 1048
  15.2 0.7 copy-done.16
  15.9 37.4 %step.1 = (bf16[96,256]{1,0:T(8,128)(2,1)S(1)}, bf16[8,48,256]{2,1,0:T(8,128)(2,1)S(1)}, bf16[8,48,256]{2,1,0:T(8,128)(2,1)S(1)}) custom-call(s32[24]{0:T(128)S(1)} %copy-done.13, s32[24]{0:T(128)S(1)} %copy-done.14, bf16[8,48,256]{2,1,0:T(8,128)(2,1)S(1)} %bitcast.7, f32[1,256]{1,0:T(1,128)S(1)} %bitcast.12, bf16[256,256]{1,0:T(8,128)(2,1)S(1)} %copy-done.6, ...), custom_call_target="tpu_custom_call" | custom-call | tf_op jit(solution)/shard_map/step/pallas_call | solution.py:658
  53.2 0.0 copy-start.4
  53.2 0.7 copy-done.4
  53.9 0.7 %copy-done.5 = bf16[8,48,256]{2,1,0:T(8,128)(2,1)} copy-done((bf16[8,48,256]{2,1,0:T(8,128)(2,1)}, bf16[8,48,256]{2,1,0:T(8,128)(2,1)S(1)}, u32[]{:S(2)}) %copy-start.5) | copy-done | bytes 196632
  54.6 0.6 copy-done.11
  55.2 11.6 %write.1 = (bf16[96,256]{1,0:T(8,128)(2,1)}, bf16[24,512,256]{2,1,0:T(8,128)(2,1)}, bf16[24,512,256]{2,1,0:T(8,128)(2,1)}) custom-call(s32[24]{0:T(128)} %prior_s.3, s32[24]{0:T(128)} %accepted_s.3, bf16[384,256]{1,0:T(8,128)(2,1)} %bitcast.8, bf16[384,256]{1,0:T(8,128)(2,1)} %bitcast.9, bf16[96,256]{1,0:T(8,128)(2,1)} %copy-done.11, ...), custom_call_target="tpu_custom_call" | custom-call | tf_op jit(solution)/shard_map/write/pallas_call | solution.py:725
  (4 shorter events, 0.0 us)
Async XLA Ops:
  0.6 2.8 %copy-start = (bf16[24,512,256]{2,1,0:T(8,128)(2,1)S(1)}, bf16[24,512,256]{2,1,0:T(8,128)(2,1)}, u32[]{:S(2)}) copy-start(bf16[24,512,256]{2,1,0:T(8,128)(2,1)} %k_ref.1) | copy-start | bytes 18874372
  3.4 2.8 %copy-start.1 = (bf16[24,512,256]{2,1,0:T(8,128)(2,1)S(1)}, bf16[24,512,256]{2,1,0:T(8,128)(2,1)}, u32[]{:S(2)}) copy-start(bf16[24,512,256]{2,1,0:T(8,128)(2,1)} %v_ref.1) | copy-start | bytes 18874372
  6.2 0.9 %copy-start.2 = (bf16[384,256]{1,0:T(8,128)(2,1)S(1)}, bf16[384,256]{1,0:T(8,128)(2,1)}, u32[]{:S(2)}) copy-start(bf16[384,256]{1,0:T(8,128)(2,1)} %param.14) | copy-start | bytes 589828
  7.1 0.9 %copy-start.3 = (f32[24,4,512]{2,1,0:T(4,128)S(1)}, f32[24,4,512]{2,1,0:T(4,128)}, u32[]{:S(2)}) copy-start(f32[24,4,512]{2,1,0:T(4,128)} %cum_hbm.1) | copy-start | bytes 589828
  8.1 0.9 %copy-start.6 = (bf16[256,256]{1,0:T(8,128)(2,1)S(1)}, bf16[256,256]{1,0:T(8,128)(2,1)}, u32[]{:S(2)}) copy-start(bf16[256,256]{1,0:T(8,128)(2,1)} %wq_ref.1) | copy-start | bytes 393220
  9.0 0.9 %copy-start.7 = (bf16[256,256]{1,0:T(8,128)(2,1)S(1)}, bf16[256,256]{1,0:T(8,128)(2,1)}, u32[]{:S(2)}) copy-start(bf16[256,256]{1,0:T(8,128)(2,1)} %wk_ref.1) | copy-start | bytes 393220
  9.9 0.9 %copy-start.8 = (bf16[256,256]{1,0:T(8,128)(2,1)S(1)}, bf16[256,256]{1,0:T(8,128)(2,1)}, u32[]{:S(2)}) copy-start(bf16[256,256]{1,0:T(8,128)(2,1)} %wv_ref.1) | copy-start | bytes 393220
  10.8 0.9 %copy-start.9 = (bf16[256,256]{1,0:T(8,128)(2,1)S(1)}, bf16[256,256]{1,0:T(8,128)(2,1)}, u32[]{:S(2)}) copy-start(bf16[256,256]{1,0:T(8,128)(2,1)} %wout_ref.1) | copy-start | bytes 393220
  11.7 0.8 %copy-start.10 = (bf16[2048,16]{0,1:T(8,128)(2,1)S(1)}, bf16[2048,16]{0,1:T(8,128)(2,1)}, u32[]{:S(2)}) copy-start(bf16[2048,16]{0,1:T(8,128)(2,1)} %param.19) | copy-start | bytes 196612
  12.5 0.7 %copy-start.12 = (s32[24,16]{0,1:T(8,128)S(1)}, s32[24,16]{0,1:T(8,128)}, u32[]{:S(2)}) copy-start(s32[24,16]{0,1:T(8,128)} %param.27) | copy-start | bytes 4612
  13.2 0.7 copy-start.13
  13.9 0.7 copy-start.14
  14.5 0.7 %copy-start.15 = (f32[256]{0:T(256)S(1)}, f32[256]{0:T(256)}, u32[]{:S(2)}) copy-start(f32[256]{0:T(256)} %param.15) | copy-start | bytes 3076
  15.2 0.7 copy-start.16
  53.2 0.7 %copy-start.4 = (bf16[8,48,256]{2,1,0:T(8,128)(2,1)}, bf16[8,48,256]{2,1,0:T(8,128)(2,1)S(1)}, u32[]{:S(2)}) copy-start(bf16[8,48,256]{2,1,0:T(8,128)(2,1)S(1)} %get-tuple-element.6) | copy-start | bytes 589828
  53.9 0.7 %copy-start.5 = (bf16[8,48,256]{2,1,0:T(8,128)(2,1)}, bf16[8,48,256]{2,1,0:T(8,128)(2,1)S(1)}, u32[]{:S(2)}) copy-start(bf16[8,48,256]{2,1,0:T(8,128)(2,1)S(1)} %get-tuple-element.7) | copy-start | bytes 589828
  54.6 0.6 copy-start.11

commit v2 on v1

--- a/solution.py
+++ b/solution.py
@@ -706,20 +706,25 @@
         ),
         name="step",
     )(
-        prior_len,
-        accepted,
-        tokens.reshape(n_chunks, rc, depth),
-        norm_gain.reshape(1, depth),
-        w_query,
-        w_key,
-        w_value,
-        w_gate.T if depth % LANES == 0 else w_gate,
-        gate_bias.reshape(1, -1),
-        w_out,
-        parents.T,
-        keys_cache,
-        values_cache,
-        cum_gates,
+        *(
+            pltpu.with_memory_space_constraint(value, pltpu.HBM)
+            for value in (
+                prior_len,
+                accepted,
+                tokens.reshape(n_chunks, rc, depth),
+                norm_gain.reshape(1, depth),
+                w_query,
+                w_key,
+                w_value,
+                w_gate.T if depth % LANES == 0 else w_gate,
+                gate_bias.reshape(1, -1),
+                w_out,
+                parents.T,
+                keys_cache,
+                values_cache,
+                cum_gates,
+            )
+        ),
     )
 
     return pl.pallas_call(
@@ -736,10 +741,11 @@
             dma((2, seq_count)),
             dma((2, seq_count)),
         ],
+        compiler_params=pltpu.CompilerParams(vmem_limit_bytes=8 * 1024 * 1024),
         name="write",
     )(
-        prior_len,
-        accepted,
+        pltpu.with_memory_space_constraint(prior_len, pltpu.HBM),
+        pltpu.with_memory_space_constraint(accepted, pltpu.HBM),
         new_keys.reshape(row_count, width),
         new_values.reshape(row_count, width),
         mixed,

time: 67.2 us -> 46.6 us (0.69)
  local copies, waits for them, and re-layouts: 17.2 us -> 0.01 us
  Pallas kernels: 48.9 us -> 45.8 us
    unnamed x34 -> x4, local copies, waits for them, and re-layouts: 17.2 us -> 0.01 us
    pallas_call x1, Pallas kernels: 11.6 us -> 7.53 us  [shards(): pl.pallas_call(write_kernel, out_shape=(jax.ShapeDtypeStruct((cpt * rc, c...]
    pallas_call x1, Pallas kernels: 37.4 us -> 38.2 us  [shards(): pl.pallas_call(functools.partial(step_kernel, n_kv, n_tp, heads, per), ou...]
where the time goes in v2:
time: 46.6 us; the launch traced here: 46.4 us
  Pallas kernels  45.8 us (98%)
  between operations  0.67 us (1%)
    pallas_call x1, Pallas kernels, shards(): pl.pallas_call(functools.partial(step_kernel, n_kv, n_tp, heads, per), ou...  38.2 us
    pallas_call x1, Pallas kernels, shards(): pl.pallas_call(write_kernel, out_shape=(jax.ShapeDtypeStruct((cpt * rc, c...  7.53 us

profile of v2, /device:TPU:5, one launch (start us, length us, event | category | flops | bytes accessed | tf_op | source)
XLA Modules:
  0.0 46.4 jit_solution(13092662392310508239)
XLA Ops:
  0.6 0.0 copy-start
  0.6 0.0 copy-start.1
  0.7 38.2 %step.1 = (bf16[96,256]{1,0:T(8,128)(2,1)S(1)}, bf16[8,48,256]{2,1,0:T(8,128)(2,1)S(1)}, bf16[8,48,256]{2,1,0:T(8,128)(2,1)S(1)}) custom-call(s32[24]{0:T(128)} %prior_s.3, s32[24]{0:T(128)} %accepted_s.3, bf16[8,48,256]{2,1,0:T(8,128)(2,1)} %bitcast.9, f32[1,256]{1,0:T(1,128)} %bitcast.12, bf16[256,256]{1,0:T(8,128)(2,1)} %wq_ref.1, ...), custom_call_target="tpu_custom_call" | custom-call | tf_op jit(solution)/shard_map/step/pallas_call | solution.py:658
  38.9 0.0 copy-done
  38.9 0.0 copy-done.1
  38.9 7.5 %write.1 = (bf16[96,256]{1,0:T(8,128)(2,1)}, bf16[24,512,256]{2,1,0:T(8,128)(2,1)}, bf16[24,512,256]{2,1,0:T(8,128)(2,1)}) custom-call(s32[24]{0:T(128)} %prior_s.3, s32[24]{0:T(128)} %accepted_s.3, bf16[384,256]{1,0:T(8,128)(2,1)S(1)} %bitcast.7, bf16[384,256]{1,0:T(8,128)(2,1)S(1)} %bitcast.8, bf16[96,256]{1,0:T(8,128)(2,1)S(1)} %get-tuple-element.8.mixed_in, ...), custom_call_target="tpu_custom_call" | custom-call | tf_op jit(solution)/shard_map/write/pallas_call | solution.py:730
Async XLA Ops:
  0.6 38.3 %copy-start = (bf16[24,512,256]{2,1,0:T(8,128)(2,1)S(1)}, bf16[24,512,256]{2,1,0:T(8,128)(2,1)}, u32[]{:S(2)}) copy-start(bf16[24,512,256]{2,1,0:T(8,128)(2,1)} %k_ref.1) | copy-start | bytes 18874372
  0.6 38.3 %copy-start.1 = (bf16[24,512,256]{2,1,0:T(8,128)(2,1)S(1)}, bf16[24,512,256]{2,1,0:T(8,128)(2,1)}, u32[]{:S(2)}) copy-start(bf16[24,512,256]{2,1,0:T(8,128)(2,1)} %v_ref.1) | copy-start | bytes 18874372

commit v3 on v2

--- a/solution.py
+++ b/solution.py
@@ -52,6 +52,21 @@
     per,
     prior_s,
     accepted_s,
+    tokens_hbm,
+    gain_hbm,
+    wq_hbm,
+    wk_hbm,
+    wv_hbm,
+    wg_hbm,
+    bias_hbm,
+    wout_hbm,
+    parents_hbm,
+    k_hbm,
+    v_hbm,
+    cum_hbm,
+    mixed_ref,
+    newk_ref,
+    newv_ref,
     tokens_ref,
     gain_ref,
     wq_ref,
@@ -61,12 +76,6 @@
     bias_ref,
     wout_ref,
     parents_ref,
-    k_hbm,
-    v_hbm,
-    cum_hbm,
-    mixed_ref,
-    newk_ref,
-    newv_ref,
     kbuf,
     vbuf,
     cumbuf,
@@ -87,6 +96,7 @@
     got_s,
     mine,
     att,
+    input_sems,
     load_sems,
     s1_send,
     s1_recv,
@@ -115,6 +125,24 @@
     corner, group = lax.rem(me, 4), me // 4
     quarter = pl.ds(corner * cq, cq)
 
+    aligned = n_tp == 4 and cpt == cq and n_kv == n_chunks
+    inputs = []
+    for at, (source, target) in enumerate(
+        (
+            (tokens_hbm, tokens_ref),
+            (wq_hbm, wq_ref),
+            (gain_hbm, gain_ref),
+            (wg_hbm, wg_ref),
+            (wk_hbm, wk_ref),
+            (wv_hbm, wv_ref),
+            (parents_hbm, parents_ref),
+            (bias_hbm, bias_ref),
+            (wout_hbm, wout_ref),
+        )
+    ):
+        copy = pltpu.make_async_copy(source, target, input_sems.at[at])
+        copy.start()
+        inputs.append(copy)
     barrier = pltpu.get_barrier_semaphore()
     for d in range(1, n_kv * n_tp):
         other = lax.rem(me * n_tp + tp + d, n_kv * n_tp)
@@ -124,13 +152,6 @@
             device_id={"kv": other // n_tp, "tp": lax.rem(other, n_tp)},
             device_id_type=MESH,
         )
-    loads = []
-    for c in range(n_chunks):
-        span = pl.ds(c * per, per)
-        for at, (source, target) in enumerate(((k_hbm, kbuf), (v_hbm, vbuf), (cum_hbm, cumbuf))):
-            copy = pltpu.make_async_copy(source.at[span], target.at[span], load_sems.at[at, c])
-            copy.start()
-            loads.append(copy)
 
     def send(source, target, sems, at, kv=None, to_tp=None):
         where = {}
@@ -149,6 +170,87 @@
         copy.start()
         return copy
 
+    for copy in inputs[:3]:
+        copy.wait()
+    floats = tokens_ref[...].reshape(n_chunks * rc, depth).astype(f32)
+    scaled = (floats * gain_ref[...]).astype(bf16)
+
+    def product(piece, w_ref):
+        value = matmul(scaled, w_ref[...]).astype(bf16)
+        part[piece] = value.reshape(n_chunks, rc, width)
+
+    product(0, wq_ref)
+    pl.semaphore_wait(barrier, n_kv * n_tp - 1)
+    started = []
+
+    def corner_sends(sources, targets, sems, piece, j=0):
+        out = []
+        for d in range(1, 4):
+            there = lax.rem(corner + d, 4)
+            at = (piece * 3 + d - 1) * cq + j
+            out.append(send(sources(there), targets(d), sems, at, kv=group * 4 + there))
+        started.extend(out)
+        return out
+
+    def first_stage(piece, j, count):
+        return corner_sends(
+            lambda there: part.at[piece, pl.ds(there * cq + j, count)],
+            lambda d: arr1.at[piece, d - 1, pl.ds(j, count)],
+            (s1_send, s1_recv),
+            piece,
+            j,
+        )
+
+    def group_sends(source, target, piece, j=0):
+        out = []
+        for d in range(1, n_groups):
+            there = lax.rem(group + d, n_groups) * 4 + corner
+            at = (piece * (n_groups - 1) + d - 1) * cq + j
+            out.append(send(source, target(d), (s2_send, s2_recv), at, kv=there))
+        started.extend(out)
+        return out
+
+    def second_stage(piece, stage, j, count):
+        for copy in stage:
+            copy.wait_recv()
+        span = pl.ds(j, count)
+        total = part[piece, pl.ds(corner * cq + j, count)].astype(f32)
+        for d in range(3):
+            total = total + arr1[piece, d, span].astype(f32)
+        half[piece, span] = total.astype(bf16)
+        return group_sends(
+            half.at[piece, span], lambda d: arr2.at[piece, d - 1, span], piece, j
+        )
+
+    def finish(piece, stage, columns, j, count):
+        for copy in stage:
+            copy.wait_recv()
+        for i in range(j, j + count):
+            total = half[piece, i].astype(f32)
+            for d in range(n_groups - 1):
+                total = total + arr2[piece, d, i].astype(f32)
+            full[piece, corner * cq + i] = (total * columns[i]).astype(bf16)
+
+    def third_stage(piece, j, count):
+        span = pl.ds(corner * cq + j, count)
+        return corner_sends(
+            lambda there: full.at[piece, span],
+            lambda d: full.at[piece, span],
+            (s3_send, s3_recv),
+            piece,
+            j,
+        )
+
+    q1 = [first_stage(0, j, 1) for j in range(cq)]
+    loads = []
+    for c in range(n_chunks):
+        span = pl.ds(c * per, per)
+        for at, (source, target) in enumerate(((k_hbm, kbuf), (v_hbm, vbuf), (cum_hbm, cumbuf))):
+            copy = pltpu.make_async_copy(source.at[span], target.at[span], load_sems.at[at, c])
+            copy.start()
+            loads.append(copy)
+    for copy in inputs[3:]:
+        copy.wait()
     total_heads = bias_ref.shape[1]
     pick = (iota((8, total_heads), 1) == tp * heads + iota((8, total_heads), 0)) & (
         iota((8, total_heads), 0) < heads
@@ -160,14 +262,6 @@
         gate_w = wg_ref[pl.ds(pl.multiple_of(me * depth, depth), depth), :]
         gate_w = contract_last(ones_where(pick, bf16), gate_w).astype(bf16)
     square_w = ones_where(iota((8, depth), 0) == SQUARE_ROW, bf16)
-    floats = tokens_ref[...].reshape(n_chunks * rc, depth).astype(f32)
-    scaled = (floats * gain_ref[...]).astype(bf16)
-
-    def product(piece, w_ref):
-        value = matmul(scaled, w_ref[...]).astype(bf16)
-        part[piece] = value.reshape(n_chunks, rc, width)
-
-    product(0, wq_ref)
     sq_hi, sq_lo = split2(floats * floats)
     gpart[...] = jnp.zeros_like(gpart)
     for c in range(n_chunks):
@@ -177,71 +271,6 @@
             + contract_last(square_w, sq_hi[rows])
             + contract_last(square_w, sq_lo[rows])
         )
-
-    pl.semaphore_wait(barrier, n_kv * n_tp - 1)
-    started = []
-
-    def corner_sends(sources, targets, sems, piece):
-        out = []
-        for d in range(1, 4):
-            there = lax.rem(corner + d, 4)
-            out.append(
-                send(
-                    sources(there), targets(d), sems, piece * 3 + d - 1, kv=group * 4 + there
-                )
-            )
-        started.extend(out)
-        return out
-
-    def first_stage(piece):
-        return corner_sends(
-            lambda there: part.at[piece, pl.ds(there * cq, cq)],
-            lambda d: arr1.at[piece, d - 1],
-            (s1_send, s1_recv),
-            piece,
-        )
-
-    def group_sends(source, target, piece):
-        out = []
-        for d in range(1, n_groups):
-            there = lax.rem(group + d, n_groups) * 4 + corner
-            out.append(
-                send(
-                    source,
-                    target(d),
-                    (s2_send, s2_recv),
-                    piece * (n_groups - 1) + d - 1,
-                    kv=there,
-                )
-            )
-        started.extend(out)
-        return out
-
-    def second_stage(piece, stage):
-        for copy in stage:
-            copy.wait_recv()
-        total = part[piece, quarter].astype(f32)
-        for d in range(3):
-            total = total + arr1[piece, d].astype(f32)
-        half[piece] = total.astype(bf16)
-        return group_sends(half.at[piece], lambda d: arr2.at[piece, d - 1], piece)
-
-    def third_stage(piece, stage, columns):
-        for copy in stage:
-            copy.wait_recv()
-        total = half[piece].astype(f32)
-        for d in range(n_groups - 1):
-            total = total + arr2[piece, d].astype(f32)
-        for j in range(cq):
-            full[piece, corner * cq + j] = (total[j] * columns[j]).astype(bf16)
-        return corner_sends(
-            lambda there: full.at[piece, quarter],
-            lambda d: full.at[piece, quarter],
-            (s3_send, s3_recv),
-            piece,
-        )
-
-    q1 = first_stage(0)
     g1 = corner_sends(
         lambda there: gpart.at[pl.ds(there * cq, cq)],
         lambda d: garr1.at[d - 1],
@@ -249,7 +278,7 @@
         3,
     )
     product(1, wk_ref)
-    k1 = first_stage(1)
+    k1 = first_stage(1, 0, cq)
     product(2, wv_ref)
 
     slot = lax.rem(me, n_tp) * cpt + me // n_tp
@@ -272,12 +301,14 @@
     for squaring in range((PROPS - 1).bit_length()):
         reached = jnp.minimum(matmul(reached.astype(bf16), reached.astype(bf16)), 1.0)
 
-    q2 = second_stage(0, q1)
+    q2 = [second_stage(0, q1[0], 0, 1)]
     for copy in g1:
         copy.wait_recv()
     ghalf[...] = gpart[quarter] + garr1[0] + garr1[1] + garr1[2]
     g2 = group_sends(ghalf, lambda d: garr2.at[d - 1], 3)
-    v1 = first_stage(2)
+    for j in range(1, cq):
+        q2.append(second_stage(0, q1[j], j, 1))
+    v1 = first_stage(2, 0, cq)
     w_copies = []
     for d in range(1, n_tp):
         w_copies.append(
@@ -313,13 +344,20 @@
                 keepdims=True,
             )
         )
-    q3 = third_stage(0, q2, [c * HEAD ** (-0.5) for c in inv_columns])
-    g3 = corner_sends(
-        lambda there: gfull.at[quarter], lambda d: gfull.at[quarter], (s3_send, s3_recv), 3
-    )
-    k2 = second_stage(1, k1)
-    v2 = second_stage(2, v1)
-
+    scaled_columns = [c * HEAD ** (-0.5) for c in inv_columns]
+    q3 = []
+    for j in range(cq):
+        finish(0, q2[j], scaled_columns, j, 1)
+        q3.append(third_stage(0, j, 1))
+    g3 = []
+    if not aligned:
+        g3 = corner_sends(
+            lambda there: gfull.at[quarter],
+            lambda d: gfull.at[quarter],
+            (s3_send, s3_recv),
+            3,
+        )
+    k2 = second_stage(1, k1, 0, cq)
     lane_head = iota((PROPS, width), 1) // HEAD
     head_rows = [ones_where(lane_head == h) for h in range(heads)]
     head_mask = jnp.concatenate(head_rows, axis=0).astype(bf16)
@@ -375,14 +413,18 @@
             parts_v[owner, k * PROPS : (k + 1) * PROPS, :] = picked.astype(bf16)
         parts_s[owner] = tile
 
-    def part_copies(d):
-        owner = lax.rem(me + d, n_kv)
+    def peer(at):
+        there = lax.rem(corner + at + jnp.where(at < n_kv - 4, 0, 1), 4)
+        return lax.rem(group + at // 4 + 1, n_groups) * 4 + there
+
+    def part_copies(at):
+        owner = peer(at)
         return [
             pltpu.make_async_remote_copy(
                 src_ref=source.at[owner],
-                dst_ref=target.at[d - 1],
-                send_sem=send_sem.at[d - 1],
-                recv_sem=recv_sem.at[d - 1],
+                dst_ref=target.at[at],
+                send_sem=send_sem.at[at],
+                recv_sem=recv_sem.at[at],
                 device_id={"kv": owner},
                 device_id_type=MESH,
             )
@@ -392,29 +434,65 @@
             )
         ]
 
-    def attend_and_send(d):
-        attend(lax.rem(me + d, n_kv))
-        for copy in part_copies(d):
+    def attend_and_send(at):
+        attend(peer(at))
+        for copy in part_copies(at):
             copy.start()
 
     for copy in loads:
         copy.wait()
-    for copy in q3:
-        copy.wait_recv()
-    attend_and_send(1)
-    k3 = third_stage(1, k2, inv_columns)
-    attend_and_send(2)
-    v3 = third_stage(2, v2, inv_columns)
-
-    def one(d, carry):
-        attend_and_send(d)
-        return carry
-
-    lax.fori_loop(3, n_kv, one, 0)
-    attend(me)
-
-    for copy in g3 + k3:
-        copy.wait_recv()
+    if aligned:
+        attend_and_send(0)
+        attend(me)
+        v2 = second_stage(2, v1, 0, cq)
+        for at in range(1, n_kv - 1):
+            if at < 4:
+                for stage in q3:
+                    stage[3 - at].wait_recv()
+            attend_and_send(at)
+    else:
+        v2 = second_stage(2, v1, 0, cq)
+        for stage in q3:
+            for copy in stage:
+                copy.wait_recv()
+
+        def one(at, carry):
+            attend_and_send(at)
+            return carry
+
+        lax.fori_loop(0, n_kv - 1, one, 0)
+        attend(me)
+    finish(1, k2, inv_columns, 0, cq)
+    finish(2, v2, inv_columns, 0, cq)
+    upper = me >= n_kv // 2
+    k3 = v3 = []
+    if aligned:
+        late = []
+        for piece in (1, 2):
+            for d in range(1, 4):
+                there = lax.rem(corner + d, 4)
+                at = (piece * 3 + d - 1) * cq
+                late.append(
+                    pltpu.make_async_remote_copy(
+                        src_ref=full.at[piece, quarter],
+                        dst_ref=full.at[piece, quarter],
+                        send_sem=s3_send.at[at],
+                        recv_sem=s3_recv.at[at],
+                        device_id={"kv": group * 4 + there},
+                        device_id_type=MESH,
+                    )
+                )
+
+        @pl.when(upper)
+        def _():
+            for copy in late:
+                copy.start()
+
+    else:
+        k3 = third_stage(1, 0, cq)
+        v3 = third_stage(2, 0, cq)
+        for copy in g3 + k3 + v3:
+            copy.wait_recv()
     gate_parts = jnp.concatenate(split3(gfull[own]), axis=0)[:, :rc].astype(bf16)
     tree_gates = contract_last(gate_parts, reached.astype(bf16))
     tree_gates = tree_gates[0:8] + tree_gates[8:16] + tree_gates[16:24]
@@ -430,15 +508,10 @@
     tree_top = jnp.max(tree, axis=1, keepdims=True)
     tree_weights = jnp.where(live, jnp.exp(tree - tree_top), 0.0)
     tree_sum = jnp.sum(tree_weights, axis=1, keepdims=True)
-    for copy in v3:
-        copy.wait_recv()
     tree_values = matmul(tree_weights.astype(bf16), full[2, own])
     tree_picked = tree_values[:rc] * wide_rows[0]
     for h in range(1, heads):
         tree_picked = tree_picked + tree_values[h * rc : (h + 1) * rc] * wide_rows[h]
-    newk_ref[...] = full[1]
-    newv_ref[...] = full[2]
-
     def tile_of(value):
         rows = [
             as_row(
@@ -457,7 +530,7 @@
 
     tree_top_tile, tree_sum_tile = tile_of(tree_top), tile_of(tree_sum)
 
-    landing = [part_copies(d) for d in range(1, n_kv)]
+    landing = [part_copies(at) for at in range(n_kv - 1)]
     for pair in landing:
         pair[1].wait_recv()
     tiles = [parts_s[me]] + [got_s[d] for d in range(n_kv - 1)]
@@ -474,32 +547,33 @@
     top = functools.reduce(jnp.maximum, tops)
     scales = [jnp.exp(t - top) for t in tops]
     total = functools.reduce(lambda a, b: a + b, [a * b for a, b in zip(scales, sums)])
+    half_lane = iota((LANES, width), 0) % (LANES // 2)
     spread = ones_where(
-        (iota((LANES, width), 0) // PROPS == iota((LANES, width), 1) // HEAD)
-        & (iota((LANES, width), 0) < lines),
-        bf16,
+        (half_lane // PROPS == iota((LANES, width), 1) // HEAD) & (half_lane < lines), bf16
     )
     fits = (iota((PROPS, LANES), 1) % PROPS == iota((PROPS, LANES), 0)) & (
-        iota((PROPS, LANES), 1) < lines
-    )
+        iota((PROPS, LANES), 1) % (LANES // 2) < lines
+    )
+    inverse = 1.0 / total
+    low_half = iota((4, LANES), 1) < LANES // 2
 
     def expand(scale):
-        scale = scale / total
+        hi, lo = split2(jnp.where(low_half, scale * inverse, 0.0))
+        both = jnp.where(low_half, hi.astype(f32), pltpu.roll(lo.astype(f32), LANES // 2, axis=1))
         rows = jnp.concatenate(
             [
-                jnp.where(fits, jnp.broadcast_to(scale[k : k + 1], (PROPS, LANES)), 0.0)
+                jnp.where(fits, jnp.broadcast_to(both[k : k + 1], (PROPS, LANES)), 0.0)
                 for k in range(per)
             ],
             axis=0,
         )
-        hi, lo = split2(rows)
-        return matmul(hi, spread) + matmul(lo, spread)
-
-    result = expand(scales[-1]) * tree_picked
-    result = result + expand(scales[0]) * parts_v[me].astype(f32)
+        return matmul(rows.astype(bf16), spread)
+
+    expanded = [expand(scale) for scale in scales]
+    result = expanded[-1] * tree_picked + expanded[0] * parts_v[me].astype(f32)
     for d in range(n_kv - 1):
         landing[d][0].wait_recv()
-        result = result + expand(scales[d + 1]) * got_v[d].astype(f32)
+        result = result + expanded[d + 1] * got_v[d].astype(f32)
     mine[...] = result.astype(bf16)
 
     target, early = lax.rem(me, n_tp), me // n_tp
@@ -551,7 +625,17 @@
         piece = matmul(rows, wall[t]).astype(bf16).astype(f32)
         mixed = piece if mixed is None else mixed + piece
     mixed_ref[...] = mixed.astype(bf16)
-
+    if aligned:
+
+        @pl.when(upper)
+        def _():
+            for copy in late:
+                copy.wait_recv()
+            for copy in late:
+                copy.wait_send()
+
+    newk_ref[...] = full[1]
+    newv_ref[...] = full[2]
     for d in range(1, n_kv):
 
         @pl.when(sends)
@@ -583,6 +667,7 @@
     windows,
     bulk_sems,
     window_sems,
+    mixed_sem,
 ):
     seq_count, length, width = k_ref.shape
     window = 2 * PROPS
@@ -593,7 +678,8 @@
             copy = pltpu.make_async_copy(source.at[b], target.at[b], bulk_sems.at[at, b])
             copy.start()
             bulk.append(copy)
-    mixed_ref[...] = mixed_in[...]
+    mixed_copy = pltpu.make_async_copy(mixed_in, mixed_ref, mixed_sem)
+    mixed_copy.start()
     placed = []
     for b in range(seq_count):
         limit = prior_s[b] + accepted_s[b] - offset
@@ -618,6 +704,7 @@
     for first, second in zip(bulk, placed):
         first.wait()
         second.start()
+    mixed_copy.wait()
     for copy in placed:
         copy.wait()
 
@@ -655,6 +742,17 @@
     hbm = pl.BlockSpec(memory_space=pltpu.HBM)
     dma = pltpu.SemaphoreType.DMA
 
+    inputs = (
+        tokens.reshape(n_chunks, rc, depth),
+        norm_gain.reshape(1, depth),
+        w_query,
+        w_key,
+        w_value,
+        w_gate.T if depth % LANES == 0 else w_gate,
+        gate_bias.reshape(1, -1),
+        w_out,
+        parents.T,
+    )
     mixed, new_keys, new_values = pl.pallas_call(
         functools.partial(step_kernel, n_kv, n_tp, heads, per),
         out_shape=(
@@ -662,9 +760,10 @@
             jax.ShapeDtypeStruct((n_chunks, rc, width), bf16),
             jax.ShapeDtypeStruct((n_chunks, rc, width), bf16),
         ),
-        in_specs=[smem] * 2 + [vmem] * 9 + [hbm] * 3,
+        in_specs=[smem] * 2 + [hbm] * 12,
         out_specs=[vmem] * 3,
-        scratch_shapes=[
+        scratch_shapes=[pltpu.VMEM(value.shape, value.dtype) for value in inputs]
+        + [
             pltpu.VMEM((seq_count, length, width), bf16),
             pltpu.VMEM((seq_count, length, width), bf16),
             pltpu.VMEM((seq_count, heads, length), f32),
@@ -685,13 +784,14 @@
             pltpu.VMEM((n_kv - 1, 8, LANES), f32),
             pltpu.VMEM((rc, width), bf16),
             pltpu.VMEM((cpt, n_tp, rc, width), bf16),
+            dma((len(inputs),)),
             dma((3, n_chunks)),
-            dma((12,)),
-            dma((12,)),
-            dma((4 * (n_groups - 1),)),
-            dma((4 * (n_groups - 1),)),
-            dma((12,)),
-            dma((12,)),
+            dma((12 * cq,)),
+            dma((12 * cq,)),
+            dma((4 * (n_groups - 1) * cq,)),
+            dma((4 * (n_groups - 1) * cq,)),
+            dma((12 * cq,)),
+            dma((12 * cq,)),
             dma((n_tp - 1,)),
             dma((n_tp - 1,)),
             dma((n_kv - 1,)),
@@ -711,15 +811,7 @@
             for value in (
                 prior_len,
                 accepted,
-                tokens.reshape(n_chunks, rc, depth),
-                norm_gain.reshape(1, depth),
-                w_query,
-                w_key,
-                w_value,
-                w_gate.T if depth % LANES == 0 else w_gate,
-                gate_bias.reshape(1, -1),
-                w_out,
-                parents.T,
+                *inputs,
                 keys_cache,
                 values_cache,
                 cum_gates,
@@ -735,11 +827,12 @@
             jax.ShapeDtypeStruct(values_cache.shape, bf16),
         ),
         in_specs=[smem] * 2 + [vmem] * 5,
-        out_specs=[vmem, hbm, hbm],
+        out_specs=[hbm, hbm, hbm],
         scratch_shapes=[
             pltpu.VMEM((2, seq_count, 2 * PROPS, width), bf16),
             dma((2, seq_count)),
             dma((2, seq_count)),
+            dma(()),
         ],
         compiler_params=pltpu.CompilerParams(vmem_limit_bytes=8 * 1024 * 1024),
         name="write",

time: 46.6 us -> 43.1 us (0.925)
  Pallas kernels: 45.8 us -> 42.3 us
    pallas_call x1, Pallas kernels: 38.2 us -> 35.4 us  [shards(): pl.pallas_call(functools.partial(step_kernel, n_kv, n_tp, heads, per), ou...]
    pallas_call x1, Pallas kernels: 7.53 us -> 6.92 us  [shards(): pl.pallas_call(write_kernel, out_shape=(jax.ShapeDtypeStruct((cpt * rc, c...]
where the time goes in v3:
time: 43.1 us; the launch traced here: 43 us
  Pallas kernels  42.3 us (98%)
  between operations  0.67 us (2%)
    pallas_call x1, Pallas kernels, shards(): pl.pallas_call(functools.partial(step_kernel, n_kv, n_tp, heads, per), ou...  35.4 us
    pallas_call x1, Pallas kernels, shards(): pl.pallas_call(write_kernel, out_shape=(jax.ShapeDtypeStruct((cpt * rc, c...  6.92 us

profile of v3, /device:TPU:5, one launch (start us, length us, event | category | flops | bytes accessed | tf_op | source)
XLA Modules:
  0.0 43.0 jit_solution(3679285206957858497)
XLA Ops:
  0.6 0.0 copy-start
  0.6 0.0 copy-start.1
  0.7 35.4 %step.1 = (bf16[96,256]{1,0:T(8,128)(2,1)S(1)}, bf16[8,48,256]{2,1,0:T(8,128)(2,1)S(1)}, bf16[8,48,256]{2,1,0:T(8,128)(2,1)S(1)}) custom-call(s32[24]{0:T(128)} %prior_s.3, s32[24]{0:T(128)} %accepted_s.3, bf16[8,48,256]{2,1,0:T(8,128)(2,1)} %bitcast.9, f32[1,256]{1,0:T(1,128)} %bitcast.12, bf16[256,256]{1,0:T(8,128)(2,1)} %wq_hbm.1, ...), custom_call_target="tpu_custom_call" | custom-call | tf_op jit(solution)/shard_map/step/pallas_call | solution.py:756
  36.0 0.0 copy-done
  36.0 0.0 copy-done.1
  36.0 6.9 %write.1 = (bf16[96,256]{1,0:T(8,128)(2,1)}, bf16[24,512,256]{2,1,0:T(8,128)(2,1)}, bf16[24,512,256]{2,1,0:T(8,128)(2,1)}) custom-call(s32[24]{0:T(128)} %prior_s.3, s32[24]{0:T(128)} %accepted_s.3, bf16[384,256]{1,0:T(8,128)(2,1)S(1)} %bitcast.7, bf16[384,256]{1,0:T(8,128)(2,1)S(1)} %bitcast.8, bf16[96,256]{1,0:T(8,128)(2,1)S(1)} %get-tuple-element.8.mixed_in, ...), custom_call_target="tpu_custom_call" | custom-call | tf_op jit(solution)/shard_map/write/pallas_call | solution.py:822
Async XLA Ops:
  0.6 35.4 %copy-start = (bf16[24,512,256]{2,1,0:T(8,128)(2,1)S(1)}, bf16[24,512,256]{2,1,0:T(8,128)(2,1)}, u32[]{:S(2)}) copy-start(bf16[24,512,256]{2,1,0:T(8,128)(2,1)} %k_ref.1) | copy-start | bytes 18874372
  0.6 35.4 %copy-start.1 = (bf16[24,512,256]{2,1,0:T(8,128)(2,1)S(1)}, bf16[24,512,256]{2,1,0:T(8,128)(2,1)}, u32[]{:S(2)}) copy-start(bf16[24,512,256]{2,1,0:T(8,128)(2,1)} %v_ref.1) | copy-start | bytes 18874372

commit v4 on v3

--- a/solution.py
+++ b/solution.py
@@ -50,8 +50,8 @@
     n_tp,
     heads,
     per,
-    prior_s,
-    accepted_s,
+    prior_hbm,
+    accepted_hbm,
     tokens_hbm,
     gain_hbm,
     wq_hbm,
@@ -76,6 +76,8 @@
     bias_ref,
     wout_ref,
     parents_ref,
+    prior_s,
+    accepted_s,
     kbuf,
     vbuf,
     cumbuf,
@@ -124,6 +126,7 @@
     cpt = n_chunks // n_tp
     corner, group = lax.rem(me, 4), me // 4
     quarter = pl.ds(corner * cq, cq)
+    order = [lax.rem(group + 1 + i, cq) for i in range(cq)]
 
     aligned = n_tp == 4 and cpt == cq and n_kv == n_chunks
     inputs = []
@@ -138,6 +141,8 @@
             (parents_hbm, parents_ref),
             (bias_hbm, bias_ref),
             (wout_hbm, wout_ref),
+            (prior_hbm, prior_s),
+            (accepted_hbm, accepted_s),
         )
     ):
         copy = pltpu.make_async_copy(source, target, input_sems.at[at])
@@ -222,14 +227,14 @@
             half.at[piece, span], lambda d: arr2.at[piece, d - 1, span], piece, j
         )
 
-    def finish(piece, stage, columns, j, count):
+    def finish(piece, stage, columns, spots):
         for copy in stage:
             copy.wait_recv()
-        for i in range(j, j + count):
-            total = half[piece, i].astype(f32)
+        for j, scale in zip(spots, columns):
+            total = half[piece, j].astype(f32)
             for d in range(n_groups - 1):
-                total = total + arr2[piece, d, i].astype(f32)
-            full[piece, corner * cq + i] = (total * columns[i]).astype(bf16)
+                total = total + arr2[piece, d, j].astype(f32)
+            full[piece, corner * cq + j] = (total * scale).astype(bf16)
 
     def third_stage(piece, j, count):
         span = pl.ds(corner * cq + j, count)
@@ -241,7 +246,7 @@
             j,
         )
 
-    q1 = [first_stage(0, j, 1) for j in range(cq)]
+    q1 = [first_stage(0, j, 1) for j in order]
     loads = []
     for c in range(n_chunks):
         span = pl.ds(c * per, per)
@@ -301,13 +306,13 @@
     for squaring in range((PROPS - 1).bit_length()):
         reached = jnp.minimum(matmul(reached.astype(bf16), reached.astype(bf16)), 1.0)
 
-    q2 = [second_stage(0, q1[0], 0, 1)]
+    q2 = [second_stage(0, q1[0], order[0], 1)]
     for copy in g1:
         copy.wait_recv()
     ghalf[...] = gpart[quarter] + garr1[0] + garr1[1] + garr1[2]
     g2 = group_sends(ghalf, lambda d: garr2.at[d - 1], 3)
-    for j in range(1, cq):
-        q2.append(second_stage(0, q1[j], j, 1))
+    for i in range(1, cq):
+        q2.append(second_stage(0, q1[i], order[i], 1))
     v1 = first_stage(2, 0, cq)
     w_copies = []
     for d in range(1, n_tp):
@@ -321,9 +326,6 @@
 
     for copy in g2:
         copy.wait_recv()
-    gates = ghalf[...]
-    for d in range(n_groups - 1):
-        gates = gates + garr2[d]
     bias = jnp.sum(
         jnp.where(pick, jnp.broadcast_to(bias_ref[...], (8, total_heads)), 0.0),
         axis=1,
@@ -331,11 +333,12 @@
     )
     inv_columns = []
     eye = iota((rc, LANES), 0) == iota((rc, LANES), 1)
-    for j in range(cq):
-        inv_row = lax.rsqrt(
-            gates[j, SQUARE_ROW : SQUARE_ROW + 1, :] / (n_kv * depth) + norm_eps
-        )
-        pre = inv_row * gates[j] + bias
+    for j in order:
+        gates = ghalf[j]
+        for d in range(n_groups - 1):
+            gates = gates + garr2[d, j]
+        inv_row = lax.rsqrt(gates[SQUARE_ROW : SQUARE_ROW + 1, :] / (n_kv * depth) + norm_eps)
+        pre = inv_row * gates + bias
         gfull[corner * cq + j] = jnp.minimum(pre, 0.0) - jnp.log1p(jnp.exp(-jnp.abs(pre)))
         inv_columns.append(
             jnp.sum(
@@ -346,9 +349,9 @@
         )
     scaled_columns = [c * HEAD ** (-0.5) for c in inv_columns]
     q3 = []
-    for j in range(cq):
-        finish(0, q2[j], scaled_columns, j, 1)
-        q3.append(third_stage(0, j, 1))
+    for i in range(cq):
+        finish(0, q2[i], scaled_columns[i : i + 1], order[i : i + 1])
+        q3.append(third_stage(0, order[i], 1))
     g3 = []
     if not aligned:
         g3 = corner_sends(
@@ -447,8 +450,9 @@
         v2 = second_stage(2, v1, 0, cq)
         for at in range(1, n_kv - 1):
             if at < 4:
-                for stage in q3:
-                    stage[3 - at].wait_recv()
+                q3[0][3 - at].wait_recv()
+            else:
+                q3[1][2 - at % 4].wait_recv()
             attend_and_send(at)
     else:
         v2 = second_stage(2, v1, 0, cq)
@@ -462,8 +466,8 @@
 
         lax.fori_loop(0, n_kv - 1, one, 0)
         attend(me)
-    finish(1, k2, inv_columns, 0, cq)
-    finish(2, v2, inv_columns, 0, cq)
+    finish(1, k2, inv_columns, order)
+    finish(2, v2, inv_columns, order)
     upper = me >= n_kv // 2
     k3 = v3 = []
     if aligned:
@@ -583,7 +587,7 @@
             dst_ref=att.at[jnp.minimum(early, cpt - 1), tp],
             send_sem=ag_send.at[d],
             recv_sem=ag_recv.at[jnp.minimum(early, cpt - 1) * n_tp + tp],
-            device_id={"kv": lax.rem(me + d, n_kv), "tp": target},
+            device_id={"kv": peer(d - 1) if d > 0 else me, "tp": target},
             device_id_type=MESH,
         )
         for d in range(n_kv)
@@ -654,8 +658,8 @@
 
 
 def write_kernel(
-    prior_s,
-    accepted_s,
+    prior_hbm,
+    accepted_hbm,
     newk_ref,
     newv_ref,
     mixed_in,
@@ -664,7 +668,10 @@
     mixed_ref,
     ko_ref,
     vo_ref,
+    prior_s,
+    accepted_s,
     windows,
+    scalar_sems,
     bulk_sems,
     window_sems,
     mixed_sem,
@@ -672,6 +679,12 @@
     seq_count, length, width = k_ref.shape
     window = 2 * PROPS
     offset = lax.axis_index("kv") * length
+    scalars = [
+        pltpu.make_async_copy(prior_hbm, prior_s, scalar_sems.at[0]),
+        pltpu.make_async_copy(accepted_hbm, accepted_s, scalar_sems.at[1]),
+    ]
+    for copy in scalars:
+        copy.start()
     bulk = []
     for b in range(seq_count):
         for at, (source, target) in enumerate(((k_ref, ko_ref), (v_ref, vo_ref))):
@@ -680,6 +693,8 @@
             bulk.append(copy)
     mixed_copy = pltpu.make_async_copy(mixed_in, mixed_ref, mixed_sem)
     mixed_copy.start()
+    for copy in scalars:
+        copy.wait()
     placed = []
     for b in range(seq_count):
         limit = prior_s[b] + accepted_s[b] - offset
@@ -738,7 +753,6 @@
     cpt = n_chunks // n_tp
     columns = w_out.shape[1]
     vmem = pl.BlockSpec(memory_space=pltpu.VMEM)
-    smem = pl.BlockSpec(memory_space=pltpu.SMEM)
     hbm = pl.BlockSpec(memory_space=pltpu.HBM)
     dma = pltpu.SemaphoreType.DMA
 
@@ -760,9 +774,10 @@
             jax.ShapeDtypeStruct((n_chunks, rc, width), bf16),
             jax.ShapeDtypeStruct((n_chunks, rc, width), bf16),
         ),
-        in_specs=[smem] * 2 + [hbm] * 12,
+        in_specs=[hbm] * 14,
         out_specs=[vmem] * 3,
         scratch_shapes=[pltpu.VMEM(value.shape, value.dtype) for value in inputs]
+        + [pltpu.SMEM((seq_count,), i32)] * 2
         + [
             pltpu.VMEM((seq_count, length, width), bf16),
             pltpu.VMEM((seq_count, length, width), bf16),
@@ -784,7 +799,7 @@
             pltpu.VMEM((n_kv - 1, 8, LANES), f32),
             pltpu.VMEM((rc, width), bf16),
             pltpu.VMEM((cpt, n_tp, rc, width), bf16),
-            dma((len(inputs),)),
+            dma((len(inputs) + 2,)),
             dma((3, n_chunks)),
             dma((12 * cq,)),
             dma((12 * cq,)),
@@ -826,10 +841,13 @@
             jax.ShapeDtypeStruct(keys_cache.shape, bf16),
             jax.ShapeDtypeStruct(values_cache.shape, bf16),
         ),
-        in_specs=[smem] * 2 + [vmem] * 5,
+        in_specs=[hbm] * 2 + [vmem] * 5,
         out_specs=[hbm, hbm, hbm],
         scratch_shapes=[
+            pltpu.SMEM((seq_count,), i32),
+            pltpu.SMEM((seq_count,), i32),
             pltpu.VMEM((2, seq_count, 2 * PROPS, width), bf16),
+            dma((2,)),
             dma((2, seq_count)),
             dma((2, seq_count)),
             dma(()),

time: 43.1 us -> 41.1 us (0.954)
  Pallas kernels: 42.3 us -> 40.2 us
    pallas_call x1, Pallas kernels: 35.4 us -> 34.2 us  [shards(): pl.pallas_call(functools.partial(step_kernel, n_kv, n_tp, heads, per), ou...]
    pallas_call x1, Pallas kernels: 6.92 us -> 6 us  [shards(): pl.pallas_call(write_kernel, out_shape=(jax.ShapeDtypeStruct((cpt * rc, c...]
where the time goes in v4:
time: 41.1 us; the launch traced here: 40.9 us
  Pallas kernels  40.2 us (98%)
  between operations  0.67 us (2%)
    pallas_call x1, Pallas kernels, shards(): pl.pallas_call(functools.partial(step_kernel, n_kv, n_tp, heads, per), ou...  34.2 us
    pallas_call x1, Pallas kernels, shards(): pl.pallas_call(write_kernel, out_shape=(jax.ShapeDtypeStruct((cpt * rc, c...  6 us

profile of v4, /device:TPU:5, one launch (start us, length us, event | category | flops | bytes accessed | tf_op | source)
XLA Modules:
  0.0 40.9 jit_solution(534902792873275766)
XLA Ops:
  0.6 0.0 copy-start
  0.6 0.0 copy-start.1
  0.7 34.2 %step.1 = (bf16[96,256]{1,0:T(8,128)(2,1)S(1)}, bf16[8,48,256]{2,1,0:T(8,128)(2,1)S(1)}, bf16[8,48,256]{2,1,0:T(8,128)(2,1)S(1)}) custom-call(s32[24]{0:T(128)} %prior_hbm.3, s32[24]{0:T(128)} %accepted_hbm.3, bf16[8,48,256]{2,1,0:T(8,128)(2,1)} %bitcast.9, f32[1,256]{1,0:T(1,128)} %bitcast.12, bf16[256,256]{1,0:T(8,128)(2,1)} %wq_hbm.1, ...), custom_call_target="tpu_custom_call" | custom-call | tf_op jit(solution)/shard_map/step/pallas_call | solution.py:770
  34.8 0.0 copy-done
  34.9 0.0 copy-done.1
  34.9 6.0 %write.1 = (bf16[96,256]{1,0:T(8,128)(2,1)}, bf16[24,512,256]{2,1,0:T(8,128)(2,1)}, bf16[24,512,256]{2,1,0:T(8,128)(2,1)}) custom-call(s32[24]{0:T(128)} %prior_hbm.3, s32[24]{0:T(128)} %accepted_hbm.3, bf16[384,256]{1,0:T(8,128)(2,1)S(1)} %bitcast.7, bf16[384,256]{1,0:T(8,128)(2,1)S(1)} %bitcast.8, bf16[96,256]{1,0:T(8,128)(2,1)S(1)} %get-tuple-element.8.mixed_in, ...), custom_call_target="tpu_custom_call" | custom-call | tf_op jit(solution)/shard_map/write/pallas_call | solution.py:837
Async XLA Ops:
  0.6 34.2 %copy-start = (bf16[24,512,256]{2,1,0:T(8,128)(2,1)S(1)}, bf16[24,512,256]{2,1,0:T(8,128)(2,1)}, u32[]{:S(2)}) copy-start(bf16[24,512,256]{2,1,0:T(8,128)(2,1)} %k_ref.1) | copy-start | bytes 18874372
  0.6 34.2 %copy-start.1 = (bf16[24,512,256]{2,1,0:T(8,128)(2,1)S(1)}, bf16[24,512,256]{2,1,0:T(8,128)(2,1)}, u32[]{:S(2)}) copy-start(bf16[24,512,256]{2,1,0:T(8,128)(2,1)} %v_ref.1) | copy-start | bytes 18874372

commit v5 on v4

--- a/solution.py
+++ b/solution.py
@@ -188,12 +188,16 @@
     pl.semaphore_wait(barrier, n_kv * n_tp - 1)
     started = []
 
+    def flip(bits):
+        low = lax.rem(corner + bits % 2, 2)
+        return lax.rem(corner // 2 + bits // 2, 2) * 2 + low
+
     def corner_sends(sources, targets, sems, piece, j=0):
-        out = []
-        for d in range(1, 4):
-            there = lax.rem(corner + d, 4)
+        out = [None] * 3
+        for d in (3, 2, 1):
+            there = flip(d)
             at = (piece * 3 + d - 1) * cq + j
-            out.append(send(sources(there), targets(d), sems, at, kv=group * 4 + there))
+            out[d - 1] = send(sources(there), targets(d), sems, at, kv=group * 4 + there)
         started.extend(out)
         return out
 
@@ -246,17 +250,9 @@
             j,
         )
 
-    q1 = [first_stage(0, j, 1) for j in order]
-    loads = []
-    for c in range(n_chunks):
-        span = pl.ds(c * per, per)
-        for at, (source, target) in enumerate(((k_hbm, kbuf), (v_hbm, vbuf), (cum_hbm, cumbuf))):
-            copy = pltpu.make_async_copy(source.at[span], target.at[span], load_sems.at[at, c])
-            copy.start()
-            loads.append(copy)
-    for copy in inputs[3:]:
-        copy.wait()
-    total_heads = bias_ref.shape[1]
+    q1 = [first_stage(0, order[0], 1)]
+    inputs[3].wait()
+    total_heads = bias_hbm.shape[1]
     pick = (iota((8, total_heads), 1) == tp * heads + iota((8, total_heads), 0)) & (
         iota((8, total_heads), 0) < heads
     )
@@ -282,6 +278,16 @@
         (s1_send, s1_recv),
         3,
     )
+    q1 = q1 + [first_stage(0, j, 1) for j in order[1:]]
+    loads = []
+    for c in range(n_chunks):
+        span = pl.ds(c * per, per)
+        for at, (source, target) in enumerate(((k_hbm, kbuf), (v_hbm, vbuf), (cum_hbm, cumbuf))):
+            copy = pltpu.make_async_copy(source.at[span], target.at[span], load_sems.at[at, c])
+            copy.start()
+            loads.append(copy)
+    for copy in inputs[4:]:
+        copy.wait()
     product(1, wk_ref)
     k1 = first_stage(1, 0, cq)
     product(2, wv_ref)
@@ -417,8 +423,12 @@
         parts_s[owner] = tile
 
     def peer(at):
-        there = lax.rem(corner + at + jnp.where(at < n_kv - 4, 0, 1), 4)
-        return lax.rem(group + at // 4 + 1, n_groups) * 4 + there
+        near = at >= n_kv - 4
+        if isinstance(at, int):
+            bits = 3 - at % 4 if near else at % 4
+        else:
+            bits = jnp.where(near, 3 - at % 4, at % 4)
+        return lax.rem(group + at // 4 + 1, n_groups) * 4 + flip(bits)
 
     def part_copies(at):
         owner = peer(at)
@@ -450,7 +460,7 @@
         v2 = second_stage(2, v1, 0, cq)
         for at in range(1, n_kv - 1):
             if at < 4:
-                q3[0][3 - at].wait_recv()
+                q3[0][at - 1].wait_recv()
             else:
                 q3[1][2 - at % 4].wait_recv()
             attend_and_send(at)
@@ -473,8 +483,8 @@
     if aligned:
         late = []
         for piece in (1, 2):
-            for d in range(1, 4):
-                there = lax.rem(corner + d, 4)
+            for d in (3, 2, 1):
+                there = flip(d)
                 at = (piece * 3 + d - 1) * cq
                 late.append(
                     pltpu.make_async_remote_copy(

time: 41.1 us -> 40.2 us (0.978)
  Pallas kernels: 40.2 us -> 39.3 us
    pallas_call x1, Pallas kernels: 34.2 us -> 33.3 us  [shards(): pl.pallas_call(functools.partial(step_kernel, n_kv, n_tp, heads, per), ou...]
where the time goes in v5:
time: 40.2 us; the launch traced here: 40 us
  Pallas kernels  39.3 us (98%)
  between operations  0.67 us (2%)
    pallas_call x1, Pallas kernels, shards(): pl.pallas_call(functools.partial(step_kernel, n_kv, n_tp, heads, per), ou...  33.3 us
    pallas_call x1, Pallas kernels, shards(): pl.pallas_call(write_kernel, out_shape=(jax.ShapeDtypeStruct((cpt * rc, c...  6 us

profile of v5, /device:TPU:5, one launch (start us, length us, event | category | flops | bytes accessed | tf_op | source)
XLA Modules:
  0.0 40.0 jit_solution(2361763896696784296)
XLA Ops:
  0.6 0.0 copy-start
  0.6 0.0 copy-start.1
  0.7 33.3 %step.1 = (bf16[96,256]{1,0:T(8,128)(2,1)S(1)}, bf16[8,48,256]{2,1,0:T(8,128)(2,1)S(1)}, bf16[8,48,256]{2,1,0:T(8,128)(2,1)S(1)}) custom-call(s32[24]{0:T(128)} %prior_hbm.3, s32[24]{0:T(128)} %accepted_hbm.3, bf16[8,48,256]{2,1,0:T(8,128)(2,1)} %bitcast.9, f32[1,256]{1,0:T(1,128)} %bitcast.12, bf16[256,256]{1,0:T(8,128)(2,1)} %wq_hbm.1, ...), custom_call_target="tpu_custom_call" | custom-call | tf_op jit(solution)/shard_map/step/pallas_call | solution.py:780
  34.0 0.0 copy-done
  34.0 0.0 copy-done.1
  34.0 6.0 %write.1 = (bf16[96,256]{1,0:T(8,128)(2,1)}, bf16[24,512,256]{2,1,0:T(8,128)(2,1)}, bf16[24,512,256]{2,1,0:T(8,128)(2,1)}) custom-call(s32[24]{0:T(128)} %prior_hbm.3, s32[24]{0:T(128)} %accepted_hbm.3, bf16[384,256]{1,0:T(8,128)(2,1)S(1)} %bitcast.7, bf16[384,256]{1,0:T(8,128)(2,1)S(1)} %bitcast.8, bf16[96,256]{1,0:T(8,128)(2,1)S(1)} %get-tuple-element.8.mixed_in, ...), custom_call_target="tpu_custom_call" | custom-call | tf_op jit(solution)/shard_map/write/pallas_call | solution.py:847
Async XLA Ops:
  0.6 33.3 %copy-start = (bf16[24,512,256]{2,1,0:T(8,128)(2,1)S(1)}, bf16[24,512,256]{2,1,0:T(8,128)(2,1)}, u32[]{:S(2)}) copy-start(bf16[24,512,256]{2,1,0:T(8,128)(2,1)} %k_ref.1) | copy-start | bytes 18874372
  0.6 33.3 %copy-start.1 = (bf16[24,512,256]{2,1,0:T(8,128)(2,1)S(1)}, bf16[24,512,256]{2,1,0:T(8,128)(2,1)}, u32[]{:S(2)}) copy-start(bf16[24,512,256]{2,1,0:T(8,128)(2,1)} %v_ref.1) | copy-start | bytes 18874372

commit v6 on v5

--- a/solution.py
+++ b/solution.py
@@ -126,7 +126,7 @@
     cpt = n_chunks // n_tp
     corner, group = lax.rem(me, 4), me // 4
     quarter = pl.ds(corner * cq, cq)
-    order = [lax.rem(group + 1 + i, cq) for i in range(cq)]
+    order = [lax.rem(group + i, cq) for i in range(cq)]
 
     aligned = n_tp == 4 and cpt == cq and n_kv == n_chunks
     inputs = []
@@ -219,7 +219,7 @@
         started.extend(out)
         return out
 
-    def second_stage(piece, stage, j, count):
+    def second_stage(piece, stage, j, count, sent=None):
         for copy in stage:
             copy.wait_recv()
         span = pl.ds(j, count)
@@ -227,6 +227,8 @@
         for d in range(3):
             total = total + arr1[piece, d, span].astype(f32)
         half[piece, span] = total.astype(bf16)
+        if sent is not None:
+            j, span = sent, pl.ds(sent, 1)
         return group_sends(
             half.at[piece, span], lambda d: arr2.at[piece, d - 1, span], piece, j
         )
@@ -355,9 +357,33 @@
         )
     scaled_columns = [c * HEAD ** (-0.5) for c in inv_columns]
     q3 = []
-    for i in range(cq):
+    first_only = order[1] if aligned else None
+    upper = me >= n_kv // 2
+    rise = [
+        pltpu.make_async_remote_copy(
+            src_ref=half.at[piece, 0],
+            dst_ref=arr2.at[piece, 0, 0],
+            send_sem=s2_send.at[piece * cq],
+            recv_sem=s2_recv.at[piece * cq],
+            device_id={"kv": lax.rem(me + 4, n_kv)},
+            device_id_type=MESH,
+        )
+        for piece in (1, 2)
+    ]
+
+    def send_up(copy):
+        @pl.when(jnp.logical_not(upper))
+        def _():
+            copy.start()
+
+    k2 = None
+    for i in list(range(1, cq)) + [0]:
         finish(0, q2[i], scaled_columns[i : i + 1], order[i : i + 1])
         q3.append(third_stage(0, order[i], 1))
+        if k2 is None:
+            k2 = second_stage(1, k1, 0, cq, first_only)
+            if aligned:
+                send_up(rise[0])
     g3 = []
     if not aligned:
         g3 = corner_sends(
@@ -366,7 +392,6 @@
             (s3_send, s3_recv),
             3,
         )
-    k2 = second_stage(1, k1, 0, cq)
     lane_head = iota((PROPS, width), 1) // HEAD
     head_rows = [ones_where(lane_head == h) for h in range(heads)]
     head_mask = jnp.concatenate(head_rows, axis=0).astype(bf16)
@@ -455,15 +480,56 @@
     for copy in loads:
         copy.wait()
     if aligned:
+        def met(piece):
+            return pltpu.make_async_remote_copy(
+                src_ref=half.at[piece, order[0]],
+                dst_ref=arr2.at[piece, 0, order[0]],
+                send_sem=s2_send.at[piece * cq + order[0]],
+                recv_sem=s2_recv.at[piece * cq + order[0]],
+                device_id={"kv": lax.rem(me + 4, n_kv)},
+                device_id_type=MESH,
+            )
+
+        late = [
+            [
+                pltpu.make_async_remote_copy(
+                    src_ref=full.at[piece, corner * cq + j],
+                    dst_ref=full.at[piece, corner * cq + j],
+                    send_sem=s3_send.at[(piece * 3 + d - 1) * cq + j],
+                    recv_sem=s3_recv.at[(piece * 3 + d - 1) * cq + j],
+                    device_id={"kv": group * 4 + flip(d)},
+                    device_id_type=MESH,
+                )
+                for piece in (1, 2)
+                for d in (3, 2, 1)
+            ]
+            for j in range(cq)
+        ]
+
+        def lift(piece):
+            rise[piece - 1].wait_recv()
+            total = half[piece, 0].astype(f32) + arr2[piece, 0, 0].astype(f32)
+            full[piece, corner * cq] = (total * inv_columns[1]).astype(bf16)
+
         attend_and_send(0)
         attend(me)
-        v2 = second_stage(2, v1, 0, cq)
+        v2 = second_stage(2, v1, 0, cq, first_only)
         for at in range(1, n_kv - 1):
             if at < 4:
                 q3[0][at - 1].wait_recv()
             else:
                 q3[1][2 - at % 4].wait_recv()
             attend_and_send(at)
+            if at == 3:
+                send_up(rise[1])
+                finish(1, [met(1)], inv_columns[:1], order[:1])
+
+                @pl.when(upper)
+                def _():
+                    lift(1)
+                    for copy in late[1][:3] + late[0][:3]:
+                        copy.start()
+
     else:
         v2 = second_stage(2, v1, 0, cq)
         for stage in q3:
@@ -476,33 +542,19 @@
 
         lax.fori_loop(0, n_kv - 1, one, 0)
         attend(me)
-    finish(1, k2, inv_columns, order)
-    finish(2, v2, inv_columns, order)
-    upper = me >= n_kv // 2
     k3 = v3 = []
     if aligned:
-        late = []
-        for piece in (1, 2):
-            for d in (3, 2, 1):
-                there = flip(d)
-                at = (piece * 3 + d - 1) * cq
-                late.append(
-                    pltpu.make_async_remote_copy(
-                        src_ref=full.at[piece, quarter],
-                        dst_ref=full.at[piece, quarter],
-                        send_sem=s3_send.at[at],
-                        recv_sem=s3_recv.at[at],
-                        device_id={"kv": group * 4 + there},
-                        device_id_type=MESH,
-                    )
-                )
+
+        finish(2, [met(2)], inv_columns[:1], order[:1])
 
         @pl.when(upper)
         def _():
-            for copy in late:
+            for copy in late[1][3:]:
                 copy.start()
 
     else:
+        finish(1, k2, inv_columns, order)
+        finish(2, v2, inv_columns, order)
         k3 = third_stage(1, 0, cq)
         v3 = third_stage(2, 0, cq)
         for copy in g3 + k3 + v3:
@@ -617,6 +669,19 @@
     def _():
         att[jnp.minimum(early, cpt - 1), tp] = mine[...]
 
+    if aligned:
+
+        @pl.when(upper)
+        def _():
+            lift(2)
+            for copy in late[0][3:]:
+                copy.start()
+
+        @pl.when(jnp.logical_not(upper))
+        def _():
+            for copy in rise:
+                copy.wait_send()
+
     for copy in w_copies:
         copy.wait_recv()
     for at in range(cpt * n_tp):
@@ -643,9 +708,9 @@
 
         @pl.when(upper)
         def _():
-            for copy in late:
+            for copy in late[1] + late[0]:
                 copy.wait_recv()
-            for copy in late:
+            for copy in late[1] + late[0]:
                 copy.wait_send()
 
     newk_ref[...] = full[1]

time: 40.2 us -> 39.9 us (level)
  no operation moved by 1% of the time
where the time goes in v6:
time: 39.9 us; the launch traced here: 39.7 us
  Pallas kernels  39 us (98%)
  between operations  0.67 us (2%)
    pallas_call x1, Pallas kernels, shards(): pl.pallas_call(functools.partial(step_kernel, n_kv, n_tp, heads, per), ou...  33 us
    pallas_call x1, Pallas kernels, shards(): pl.pallas_call(write_kernel, out_shape=(jax.ShapeDtypeStruct((cpt * rc, c...  6 us

profile of v6, /device:TPU:5, one launch (start us, length us, event | category | flops | bytes accessed | tf_op | source)
XLA Modules:
  0.0 39.7 jit_solution(10264487745868609763)
XLA Ops:
  0.6 0.0 copy-start
  0.6 0.0 copy-start.1
  0.7 33.0 %step.1 = (bf16[96,256]{1,0:T(8,128)(2,1)S(1)}, bf16[8,48,256]{2,1,0:T(8,128)(2,1)S(1)}, bf16[8,48,256]{2,1,0:T(8,128)(2,1)S(1)}) custom-call(s32[24]{0:T(128)} %prior_hbm.3, s32[24]{0:T(128)} %accepted_hbm.3, bf16[8,48,256]{2,1,0:T(8,128)(2,1)} %bitcast.9, f32[1,256]{1,0:T(1,128)} %bitcast.12, bf16[256,256]{1,0:T(8,128)(2,1)} %wq_hbm.1, ...), custom_call_target="tpu_custom_call" | custom-call | tf_op jit(solution)/shard_map/step/pallas_call | solution.py:845
  33.7 0.0 copy-done
  33.7 0.0 copy-done.1
  33.7 6.0 %write.1 = (bf16[96,256]{1,0:T(8,128)(2,1)}, bf16[24,512,256]{2,1,0:T(8,128)(2,1)}, bf16[24,512,256]{2,1,0:T(8,128)(2,1)}) custom-call(s32[24]{0:T(128)} %prior_hbm.3, s32[24]{0:T(128)} %accepted_hbm.3, bf16[384,256]{1,0:T(8,128)(2,1)S(1)} %bitcast.7, bf16[384,256]{1,0:T(8,128)(2,1)S(1)} %bitcast.8, bf16[96,256]{1,0:T(8,128)(2,1)S(1)} %get-tuple-element.8.mixed_in, ...), custom_call_target="tpu_custom_call" | custom-call | tf_op jit(solution)/shard_map/write/pallas_call | solution.py:912
Async XLA Ops:
  0.6 33.1 %copy-start = (bf16[24,512,256]{2,1,0:T(8,128)(2,1)S(1)}, bf16[24,512,256]{2,1,0:T(8,128)(2,1)}, u32[]{:S(2)}) copy-start(bf16[24,512,256]{2,1,0:T(8,128)(2,1)} %k_ref.1) | copy-start | bytes 18874372
  0.6 33.1 %copy-start.1 = (bf16[24,512,256]{2,1,0:T(8,128)(2,1)S(1)}, bf16[24,512,256]{2,1,0:T(8,128)(2,1)}, u32[]{:S(2)}) copy-start(bf16[24,512,256]{2,1,0:T(8,128)(2,1)} %v_ref.1) | copy-start | bytes 18874372

commit v7 on v6

--- a/solution.py
+++ b/solution.py
@@ -158,7 +158,7 @@
             device_id_type=MESH,
         )
 
-    def send(source, target, sems, at, kv=None, to_tp=None):
+    def send(source, target, sems, at, kv=None, to_tp=None, out=None):
         where = {}
         if kv is not None:
             where["kv"] = kv
@@ -167,7 +167,7 @@
         copy = pltpu.make_async_remote_copy(
             src_ref=source,
             dst_ref=target,
-            send_sem=sems[0].at[at],
+            send_sem=sems[0].at[at if out is None else out],
             recv_sem=sems[1].at[at],
             device_id=where,
             device_id_type=MESH,
@@ -187,6 +187,17 @@
     product(0, wq_ref)
     pl.semaphore_wait(barrier, n_kv * n_tp - 1)
     started = []
+
+    def sent(like, sem):
+        pltpu.make_async_remote_copy(
+            src_ref=like,
+            dst_ref=like,
+            send_sem=sem,
+            recv_sem=s1_recv.at[0],
+            device_id={"kv": lax.rem(me + 1, n_kv)},
+            device_id_type=MESH,
+        ).wait_send()
+
 
     def flip(bits):
         low = lax.rem(corner + bits % 2, 2)
@@ -197,8 +208,9 @@
         for d in (3, 2, 1):
             there = flip(d)
             at = (piece * 3 + d - 1) * cq + j
-            out[d - 1] = send(sources(there), targets(d), sems, at, kv=group * 4 + there)
-        started.extend(out)
+            out[d - 1] = send(
+                sources(there), targets(d), sems, at, kv=group * 4 + there, out=piece
+            )
         return out
 
     def first_stage(piece, j, count):
@@ -282,12 +294,10 @@
     )
     q1 = q1 + [first_stage(0, j, 1) for j in order[1:]]
     loads = []
-    for c in range(n_chunks):
-        span = pl.ds(c * per, per)
-        for at, (source, target) in enumerate(((k_hbm, kbuf), (v_hbm, vbuf), (cum_hbm, cumbuf))):
-            copy = pltpu.make_async_copy(source.at[span], target.at[span], load_sems.at[at, c])
-            copy.start()
-            loads.append(copy)
+    for at, (source, target) in enumerate(((k_hbm, kbuf), (v_hbm, vbuf), (cum_hbm, cumbuf))):
+        copy = pltpu.make_async_copy(source, target, load_sems.at[at])
+        copy.start()
+        loads.append(copy)
     for copy in inputs[4:]:
         copy.wait()
     product(1, wk_ref)
@@ -461,7 +471,7 @@
             pltpu.make_async_remote_copy(
                 src_ref=source.at[owner],
                 dst_ref=target.at[at],
-                send_sem=send_sem.at[at],
+                send_sem=send_sem,
                 recv_sem=recv_sem.at[at],
                 device_id={"kv": owner},
                 device_id_type=MESH,
@@ -495,7 +505,7 @@
                 pltpu.make_async_remote_copy(
                     src_ref=full.at[piece, corner * cq + j],
                     dst_ref=full.at[piece, corner * cq + j],
-                    send_sem=s3_send.at[(piece * 3 + d - 1) * cq + j],
+                    send_sem=s3_send.at[piece],
                     recv_sem=s3_recv.at[(piece * 3 + d - 1) * cq + j],
                     device_id={"kv": group * 4 + flip(d)},
                     device_id_type=MESH,
@@ -710,8 +720,8 @@
         def _():
             for copy in late[1] + late[0]:
                 copy.wait_recv()
-            for copy in late[1] + late[0]:
-                copy.wait_send()
+            for piece in (1, 2):
+                sent(arr1.at[piece], s3_send.at[piece])
 
     newk_ref[...] = full[1]
     newv_ref[...] = full[2]
@@ -725,11 +735,18 @@
     def _():
         spreads[0].wait_send()
 
+    for piece in range(3):
+        sent(arr1.at[piece], s1_send.at[piece])
+    sent(garr1, s1_send.at[3])
+    sent(arr1.at[0], s3_send.at[0])
+    if not aligned:
+        sent(arr1.at[1], s3_send.at[1])
+        sent(arr1.at[2], s3_send.at[2])
+        sent(garr1, s3_send.at[3])
     for copy in started:
         copy.wait_send()
-    for pair in landing:
-        for copy in pair:
-            copy.wait_send()
+    sent(got_v, cv_send)
+    sent(got_s, cs_send)
 
 
 def write_kernel(
@@ -761,11 +778,21 @@
     for copy in scalars:
         copy.start()
     bulk = []
+    block = next(n for n in (3, 2, 1) if seq_count % n == 0)
     for b in range(seq_count):
         for at, (source, target) in enumerate(((k_ref, ko_ref), (v_ref, vo_ref))):
-            copy = pltpu.make_async_copy(source.at[b], target.at[b], bulk_sems.at[at, b])
+            copy = pltpu.make_async_copy(
+                source.at[b], target.at[b], bulk_sems.at[at, b // block]
+            )
             copy.start()
-            bulk.append(copy)
+    for first in range(0, seq_count, block):
+        span = pl.ds(first, block)
+        for at, (source, target) in enumerate(((k_ref, ko_ref), (v_ref, vo_ref))):
+            bulk.append(
+                pltpu.make_async_copy(
+                    source.at[span], target.at[span], bulk_sems.at[at, first // block]
+                )
+            )
     mixed_copy = pltpu.make_async_copy(mixed_in, mixed_ref, mixed_sem)
     mixed_copy.start()
     for copy in scalars:
@@ -788,15 +815,17 @@
                 pltpu.make_async_copy(
                     windows.at[at, b],
                     target.at[b, pl.ds(start, window), :],
-                    window_sems.at[at, b],
+                    window_sems.at[at],
                 )
             )
-    for first, second in zip(bulk, placed):
-        first.wait()
-        second.start()
+    for at, copy in enumerate(bulk):
+        copy.wait()
+        base = at // 2 * 2 * block + at % 2
+        for second in placed[base : base + 2 * block : 2]:
+            second.start()
     mixed_copy.wait()
-    for copy in placed:
-        copy.wait()
+    for at in range(2):
+        pltpu.make_async_copy(windows.at[at], windows.at[at], window_sems.at[at]).wait()
 
 
 def shards(
@@ -875,18 +904,18 @@
             pltpu.VMEM((rc, width), bf16),
             pltpu.VMEM((cpt, n_tp, rc, width), bf16),
             dma((len(inputs) + 2,)),
-            dma((3, n_chunks)),
-            dma((12 * cq,)),
+            dma((3,)),
+            dma((4,)),
             dma((12 * cq,)),
             dma((4 * (n_groups - 1) * cq,)),
             dma((4 * (n_groups - 1) * cq,)),
-            dma((12 * cq,)),
+            dma((4,)),
             dma((12 * cq,)),
             dma((n_tp - 1,)),
             dma((n_tp - 1,)),
+            dma(()),
             dma((n_kv - 1,)),
-            dma((n_kv - 1,)),
-            dma((n_kv - 1,)),
+            dma(()),
             dma((n_kv - 1,)),
             dma((n_kv,)),
             dma((cpt * n_tp,)),
@@ -923,8 +952,8 @@
             pltpu.SMEM((seq_count,), i32),
             pltpu.VMEM((2, seq_count, 2 * PROPS, width), bf16),
             dma((2,)),
-            dma((2, seq_count)),
-            dma((2, seq_count)),
+            dma((2, seq_count // next(n for n in (3, 2, 1) if seq_count % n == 0))),
+            dma((2,)),
             dma(()),
         ],
         compiler_params=pltpu.CompilerParams(vmem_limit_bytes=8 * 1024 * 1024),

time: 39.9 us -> 38.5 us (0.965)
  Pallas kernels: 39 us -> 37.6 us
    pallas_call x1, Pallas kernels: 33 us -> 32.3 us  [shards(): pl.pallas_call(functools.partial(step_kernel, n_kv, n_tp, heads, per), ou...]
    pallas_call x1, Pallas kernels: 6 us -> 5.31 us  [shards(): pl.pallas_call(write_kernel, out_shape=(jax.ShapeDtypeStruct((cpt * rc, c...]
where the time goes in v7:
time: 38.5 us; the launch traced here: 38.3 us
  Pallas kernels  37.6 us (98%)
  between operations  0.67 us (2%)
    pallas_call x1, Pallas kernels, shards(): pl.pallas_call(functools.partial(step_kernel, n_kv, n_tp, heads, per), ou...  32.3 us
    pallas_call x1, Pallas kernels, shards(): pl.pallas_call(write_kernel, out_shape=(jax.ShapeDtypeStruct((cpt * rc, c...  5.31 us

profile of v7, /device:TPU:5, one launch (start us, length us, event | category | flops | bytes accessed | tf_op | source)
XLA Modules:
  0.0 38.3 jit_solution(12730129946058345601)
XLA Ops:
  0.6 0.0 copy-start
  0.6 0.0 copy-start.1
  0.7 32.3 %step.1 = (bf16[96,256]{1,0:T(8,128)(2,1)S(1)}, bf16[8,48,256]{2,1,0:T(8,128)(2,1)S(1)}, bf16[8,48,256]{2,1,0:T(8,128)(2,1)S(1)}) custom-call(s32[24]{0:T(128)} %prior_hbm.3, s32[24]{0:T(128)} %accepted_hbm.3, bf16[8,48,256]{2,1,0:T(8,128)(2,1)} %bitcast.9, f32[1,256]{1,0:T(1,128)} %bitcast.12, bf16[256,256]{1,0:T(8,128)(2,1)} %wq_hbm.1, ...), custom_call_target="tpu_custom_call" | custom-call | tf_op jit(solution)/shard_map/step/pallas_call | solution.py:874
  33.0 0.0 copy-done
  33.0 0.0 copy-done.1
  33.0 5.3 %write.1 = (bf16[96,256]{1,0:T(8,128)(2,1)}, bf16[24,512,256]{2,1,0:T(8,128)(2,1)}, bf16[24,512,256]{2,1,0:T(8,128)(2,1)}) custom-call(s32[24]{0:T(128)} %prior_hbm.3, s32[24]{0:T(128)} %accepted_hbm.3, bf16[384,256]{1,0:T(8,128)(2,1)S(1)} %bitcast.7, bf16[384,256]{1,0:T(8,128)(2,1)S(1)} %bitcast.8, bf16[96,256]{1,0:T(8,128)(2,1)S(1)} %get-tuple-element.8.mixed_in, ...), custom_call_target="tpu_custom_call" | custom-call | tf_op jit(solution)/shard_map/write/pallas_call | solution.py:941
Async XLA Ops:
  0.6 32.4 %copy-start = (bf16[24,512,256]{2,1,0:T(8,128)(2,1)S(1)}, bf16[24,512,256]{2,1,0:T(8,128)(2,1)}, u32[]{:S(2)}) copy-start(bf16[24,512,256]{2,1,0:T(8,128)(2,1)} %k_ref.1) | copy-start | bytes 18874372
  0.6 32.4 %copy-start.1 = (bf16[24,512,256]{2,1,0:T(8,128)(2,1)S(1)}, bf16[24,512,256]{2,1,0:T(8,128)(2,1)}, u32[]{:S(2)}) copy-start(bf16[24,512,256]{2,1,0:T(8,128)(2,1)} %v_ref.1) | copy-start | bytes 18874372
